TPU v7x, 1024 devices: a 2x16x16 block of a 4x16x16 slice. The times are simulated.
1024 devices in a mesh: grp: 2 (over x), row: 16 (over z), col: 32 (over y, core).
Axes of the slice: x: 2, y: 16, z: 16, core: 2. Of those that a mesh axis runs over, the one named last changes fastest.
The devices are a block of a 4x16x16 slice.
Arguments:
- gate_in: bfloat16 [32, 4096, 1024], P(('grp', 'row'), 'col'), parts along dimension 0, may hold values from -6 to 6
- mult_in: bfloat16 [32, 4096, 1024], P(('grp', 'row'), 'col'), parts along dimension 0, may hold values from -6 to 6
- value_in: bfloat16 [32, 4096, 1024], P(('grp', 'row'), 'col'), parts along dimension 0, may hold values from -6 to 6
- taps_gate: float32 [3, 1024], replicated, may hold values from -3.5 to 3.5
- taps_mult: float32 [3, 1024], replicated, may hold values from -3.5 to 3.5
- taps_value: float32 [3, 1024], replicated, may hold values from -3.5 to 3.5
- filter_first: float32 [33, 128], replicated, may hold values from -3 to 3
- filter_second: float32 [128, 128], replicated, may hold values from -1 to 1
- filter_ahead: float32 [128, 1024], replicated, may hold values from -0.5 to 0.5
- filter_behind: float32 [128, 1024], replicated, may hold values from -0.5 to 0.5
- filter_decay: float32 [1024], replicated, may hold values from 0.05 to 136.5
- skip_gain: float32 [1024], replicated, may hold values from -5 to 5
- out_weight: bfloat16 [1024, 2048], replicated, may hold values from -0.1875 to 0.1875
Outputs:
- mixed: bfloat16 [32, 4096, 2048], P(('grp', 'row'), 'col'), parts along dimension 0
There are 2 independent parts, one for each index of `grp`. A program takes and returns all parts, laid end to end along the dimension named above; an argument that names none is the same for every part. Nothing has to cross between parts.
All inputs are finite; a program needn't handle non-finite values.
Results may differ from a plain program's by a relative error of at most 0.0049.
Values may be sent and summed in bfloat16 or wider, within the bound.
No kernel may reach another device: no remote copies, remote signals or barrier semaphores. Data moves between devices by JAX's collectives and lax.ppermute only.
A program may use at most 32 MiB of HBM per device.

v0:
```python
import math

import jax
import jax.numpy as jnp
from jax import lax
from jax.sharding import Mesh
from jax.sharding import PartitionSpec as P

COL = ("col_0", "col_1")


highest = lax.Precision.HIGHEST


def padded_2(shard, sides, width):
    for axis, dim in sides:
        size, length = (lax.axis_size(axis), shard.shape[dim])
        up = [(i, (i + 1) % size) for i in range(size - 1)]
        down = [(j, i) for i, j in up]
        last = lax.slice_in_dim(shard, length - width, length, axis=dim)
        leading = lax.slice_in_dim(shard, 0, width, axis=dim)
        before = lax.ppermute(last, axis, up)
        after = lax.ppermute(leading, axis, down)
        shard = jnp.concatenate([before, shard, after], axis=dim)
    return shard


def cut_along(shard, dim, size):
    before, after = (shard.shape[:dim], shard.shape[dim + 1 :])
    return jnp.moveaxis(shard.reshape(*before, size, -1, *after), dim, 0)


def laid_out(blocks, dim):
    lengths = list(blocks.shape[1:])
    lengths[dim] *= blocks.shape[0]
    return jnp.moveaxis(blocks, 0, dim).reshape(lengths)


def moved_by_axis(blocks, axes, turns):
    inside = blocks.shape[1:]
    result = blocks.reshape(*(lax.axis_size(a) for a in axes), *inside)
    for k in turns:
        result = lax.all_to_all(result, axes[k], k, k, tiled=True)
    return result.reshape(-1, *inside)


def exchange_by_chip(shard, groups, turns, split_dim, concat_dim):
    size = lax.axis_size(groups[0]) * lax.axis_size(groups[1])
    blocks = cut_along(shard, split_dim, size)
    return laid_out(moved_by_axis(blocks, groups, turns), concat_dim)


def filter_hidden(mirror, seq_len, filter_first, filter_second):
    tau_values = mirror.astype(jnp.float32) / (seq_len - 1)
    omega_pos = 2.0 * math.pi / seq_len * mirror.astype(jnp.float32)
    band_count = (filter_first.shape[0] - 1) // 2
    band_values = jnp.linspace(0.0001, band_count - 1, band_count, dtype=jnp.float32)
    angles = omega_pos[:, None] * band_values[None, :]
    features = jnp.concatenate([tau_values[:, None], jnp.cos(angles), -jnp.sin(angles)], axis=1)
    hidden = jnp.sin(jnp.dot(features, filter_first, precision=highest))
    hidden = jnp.sin(jnp.dot(hidden, filter_second, precision=highest))
    return (hidden, tau_values)


def side_values(hidden, tau_values, side_weight, decay_rates):
    values = jnp.einsum("pf,fh->hp", hidden, side_weight, precision=highest)
    return values * jnp.exp(-decay_rates[:, None] * tau_values[None, :])


def angle_table(row_count, column_count, period):
    products = (
        lax.iota(jnp.int32, row_count)[:, None]
        * lax.iota(jnp.int32, column_count)[None, :]
        % period
    )
    angle = products.astype(jnp.float32) * (2.0 * math.pi / period)
    return (jnp.cos(angle), jnp.sin(angle))


def swap_halves(stacked, width):
    return jnp.concatenate([stacked[..., width:], stacked[..., :width]], axis=-1)


def forward(values, first_table, twist_even, twist_odd, second_block):
    channels, _, width = values.shape
    first = jnp.einsum("sfa,cab->cfsb", first_table, values, precision=highest)
    first = first.reshape(channels, first_table.shape[1], 2 * width)
    turned = first * twist_even + swap_halves(first, width) * twist_odd
    return jnp.einsum("cfk,kl->cfl", turned, second_block, precision=highest)


def inverse(spectrum, last_table, twist_even, twist_odd, second_block, span_len):
    channels, freq_rows, double_width = spectrum.shape
    width = double_width // 2
    back = jnp.einsum("cfk,kl->cfl", spectrum, second_block, precision=highest)
    turned = back * twist_even + swap_halves(back, width) * twist_odd
    turned = turned.reshape(channels, freq_rows, 2, width)
    result = jnp.einsum("asf,cfsb->cab", last_table, turned, precision=highest)
    return result / span_len


def body(
    gate_in,
    mult_in,
    value_in,
    taps_gate,
    taps_mult,
    taps_value,
    filter_first,
    filter_second,
    filter_ahead,
    filter_behind,
    filter_decay,
    skip_gain,
    out_weight,
):
    col_count = lax.axis_size(COL)
    col_index = lax.axis_index(COL)
    tok_rows = gate_in.shape[1]
    seq_len = tok_rows * col_count
    span_len = 2 * seq_len
    group_size = filter_ahead.shape[1] // col_count
    stacked = jnp.stack([gate_in[0], mult_in[0], value_in[0]])
    padded = padded_2(stacked, ((COL, 1),), 1).astype(jnp.float32)
    all_taps = jnp.stack([taps_gate, taps_mult, taps_value])
    shorted = jnp.zeros(stacked.shape, jnp.float32)
    for offset in range(all_taps.shape[1]):
        shorted = shorted + all_taps[:, offset][:, None, :] * padded[:, offset : offset + tok_rows]
    gate_part = shorted[0]
    product = shorted[2] * shorted[1]
    spread = lax.all_to_all(product.T, COL, split_axis=0, concat_axis=1, tiled=True)
    first_channel = col_index * group_size
    own_rates = lax.dynamic_slice_in_dim(filter_decay, first_channel, group_size)
    mirror = lax.iota(jnp.int32, seq_len)
    hidden, tau_values = filter_hidden(mirror, seq_len, filter_first, filter_second)
    ahead_vals = side_values(
        hidden,
        tau_values,
        lax.dynamic_slice_in_dim(filter_ahead, first_channel, group_size, 1),
        own_rates,
    )
    behind_vals = side_values(
        hidden,
        tau_values,
        lax.dynamic_slice_in_dim(filter_behind, first_channel, group_size, 1),
        own_rates,
    )
    kernel = jnp.concatenate(
        [ahead_vals, jnp.zeros((group_size, 1), jnp.float32), jnp.flip(behind_vals[:, 1:], axis=1)],
        axis=1,
    )
    kernel = kernel * lax.rsqrt(jnp.sum(kernel * kernel, axis=1, keepdims=True) + 1e-06)
    factor = 128
    half_rows = factor // 2
    width_second = span_len // factor
    first_cos, first_sin = angle_table(factor, factor, factor)
    twist_cos, twist_sin = angle_table(factor, width_second, span_len)
    second_cos, second_sin = angle_table(width_second, width_second, width_second)
    first_table = jnp.stack([first_cos, -first_sin])
    last_table = jnp.stack([first_cos[:half_rows], -first_sin[:half_rows]], axis=1)
    twist_even = jnp.concatenate([twist_cos, twist_cos], axis=1)
    twist_ahead = jnp.concatenate([twist_sin, -twist_sin], axis=1)
    twist_back = jnp.concatenate([-twist_sin, twist_sin], axis=1)
    block_ahead = jnp.concatenate(
        [
            jnp.concatenate([second_cos, -second_sin], axis=1),
            jnp.concatenate([second_sin, second_cos], axis=1),
        ],
        axis=0,
    )
    block_back = jnp.concatenate(
        [
            jnp.concatenate([second_cos, second_sin], axis=1),
            jnp.concatenate([-second_sin, second_cos], axis=1),
        ],
        axis=0,
    )
    kernel_spec = forward(
        kernel.reshape(group_size, factor, width_second),
        first_table,
        twist_even,
        twist_ahead,
        block_ahead,
    )
    data_spec = forward(
        spread.reshape(group_size, half_rows, width_second),
        first_table[:, :, :half_rows],
        twist_even,
        twist_ahead,
        block_ahead,
    )
    data_re = data_spec[..., :width_second]
    data_im = data_spec[..., width_second:]
    kernel_re = kernel_spec[..., :width_second]
    kernel_im = kernel_spec[..., width_second:]
    joined = jnp.concatenate(
        [data_re * kernel_re - data_im * kernel_im, data_re * kernel_im + data_im * kernel_re],
        axis=-1,
    )
    convolved = inverse(joined, last_table, twist_even, twist_back, block_back, span_len).reshape(
        group_size, seq_len
    )
    returned = exchange_by_chip(convolved, ("col_0", "col_1"), (1, 0), 1, 0)
    mixed_rows = ((returned.T + skip_gain * product) * gate_part).astype(jnp.bfloat16)
    return jnp.dot(mixed_rows, out_weight, preferred_element_type=jnp.float32).astype(jnp.bfloat16)[
        None
    ]


def solution(mesh):
    split = Mesh(
        mesh.devices.reshape(mesh.shape["grp"], mesh.shape["row"], 16, 2),
        ("grp", "row", "col_0", "col_1"),
    )
    in_specs = (
        P(("grp", "row"), COL, None),
        P(("grp", "row"), COL, None),
        P(("grp", "row"), COL, None),
        P(),
        P(),
        P(),
        P(),
        P(),
        P(),
        P(),
        P(),
        P(),
        P(),
    )
    out_specs = P(("grp", "row"), COL, None)
    return jax.shard_map(body, mesh=split, in_specs=in_specs, out_specs=out_specs, check_vma=False)
```

profile of v0, /device:TPU:12, one launch (start us, length us, event | category | flops | bytes accessed | tf_op | source)
XLA Modules:
  0.0 219.8 jit_solution(15049787146190918876)
XLA Ops:
  0.0 1.2 copy.31
  1.2 1.1 copy.32
  2.3 1.1 copy.33
  3.4 0.1 pad_maximum_fusion
  3.5 0.0 copy-start.6
  3.5 0.3 fusion.104
  3.8 0.4 copy.34
  4.2 2.0 collective-permute-start
  6.2 0.0 copy-start.5
  6.2 0.4 copy.35
  6.6 3.7 %collective-permute-start.1 = (bf16[3,1,1024]{2,0,1:T(4,128)(2,1)S(1)}, bf16[3,1,1024]{2,0,1:T(4,128)(2,1)}, u32[]{:S(2)}, u32[]{:S(2)}) collective-permute-start(bf16[3,1,1024]{2,0,1:T(4,128)(2,1)S(1)} %copy.35), channel_id=1, source_target_pairs={{1,0},{2,1},{3,2},{4,3},{5,4},{6,5},{7,6},{8,7},{9,8},{10,9},{11,1... | collective-permute-start | bytes 18440 | tf_op jit(solution)/shard_map/ppermute | solution.py:23
  10.3 0.8 fusion.86
  11.1 0.1 fusion.84
  11.2 0.1 pad_maximum_fusion.14
  11.3 1.0 multiply_cosine_fusion
  12.3 10.9 %convolution_sine_fusion.1 = f32[4096,128]{1,0:T(8,128)S(1)} fusion(f32[33,128]{1,0:T(8,128)S(1)} %copy-done.6, f32[4096,16]{0,1:T(8,128)S(1)} %get-tuple-element.23, f32[4096,16]{0,1:T(8,128)S(1)} %get-tuple-element.22, f32[4096,1]{0,1:T(1,128)S(1)} %convert_multiply_fusion.2), kind=kOutput, calls=%fused_computation.1 | convolution fusion | flops 207888384 | bytes 2654720 | tf_op jit(solution)/shard_map/dot_general | solution.py:60
  23.2 9.4 %convolution_sine_fusion = f32[4096,128]{1,0:T(8,128)S(1)} fusion(f32[4096,128]{1,0:T(8,128)S(1)} %convolution_sine_fusion.1, f32[128,128]{1,0:T(8,128)S(1)} %copy-done.5), kind=kOutput, calls=%fused_computation | convolution fusion | flops 805306368 | bytes 4259840 | tf_op jit(solution)/shard_map/dot_general | solution.py:61
  32.6 0.8 dynamic-slice_negate_fusion
  33.4 2.3 %fusion.62 = f32[32,4096]{1,0:T(8,128)S(1)} fusion(f32[4096,128]{1,0:T(8,128)S(1)} %convolution_sine_fusion, f32[128,1024]{1,0:T(8,128)S(1)} %copy-done, s32[]{:T(128)S(6)} %select_n.68), kind=kOutput, calls=%fused_computation.98 | convolution fusion | flops 201326592 | bytes 2686980 | tf_op jit(solution)/shard_map/pf,fh->hp/dot_general | solution.py:66
  35.7 0.1 multiply_exponential_fusion
  35.8 0.0 copy-start.8
  35.8 0.0 copy-start.9
  35.9 3.9 %convolution_multiply_fusion = f32[32,4096]{1,0:T(8,128)} fusion(f32[4096,128]{1,0:T(8,128)S(1)} %convolution_sine_fusion, f32[4096]{0:T(1024)S(1)} %convert_multiply_fusion, f32[32]{0:T(128)S(1)} %dynamic-slice_negate_fusion, f32[128,1024]{1,0:T(8,128)} %param.21, s32[]{:T(128)S(6)} %select_n.68), kind=kOutput, calls=%fused_computation.2 | convolution fusion | flops 201588736 | bytes 2703492 | tf_op jit(solution)/shard_map/pf,fh->hp/dot_general | solution.py:66
  39.8 0.3 slice_multiply_fusion.3
  40.2 0.1 fusion.87
  40.4 0.4 copy.36
  40.8 1.1 copy.37
  41.9 0.8 maximum_convert_fusion
  42.8 2.3 %fusion.21 = f32[3,128,1024]{1,2,0:T(8,128)S(1)} fusion(f32[3,130,1024]{1,2,0:T(8,128)S(1)} %maximum_convert_fusion, f32[3,1024]{1,0:T(4,128)S(1)} %get-tuple-element.24, f32[3,1024]{1,0:T(4,128)S(1)} %get-tuple-element.25, f32[3,1024]{1,0:T(4,128)S(1)} %bitcast.98), kind=kLoop, calls=%fused_computation.27 | loop fusion | flops 1966080 | bytes 6328320 | tf_op jit(solution)/shard_map/add | solution.py:128
  45.1 0.8 slice_multiply_fusion.4
  46.0 83.7 %all-to-all-start = ((f32[32,32,128]{2,1,0:T(8,128)}), f32[32,32,128]{2,1,0:T(8,128)}, u32[]{:S(2)}, u32[]{:S(2)}) async-start(f32[32,32,128]{2,1,0:T(8,128)} %bitcast.5), calls=%async_computation | async-start | bytes 1048576 | tf_op jit(solution)/shard_map/all_to_all | solution.py:131
  129.7 0.1 fusion.89
  129.8 2.3 %reverse = f32[32,4096]{1,0:T(8,128)S(1)} reverse(f32[32,4096]{1,0:T(8,128)S(1)} %bitcast.96), dimensions={1} | reverse | bytes 1048576
  132.1 1.1 slice.164
  133.2 1.6 concatenate.63
  134.8 2.2 concatenate.64
  137.0 0.3 sine_negate_fusion
  137.3 1.5 pad_maximum_fusion.9
  138.8 0.2 multiply_reduce_fusion
  139.0 0.7 cosine_bitcast_fusion
  139.7 5.2 %fusion.16 = f32[32,64,2,128]{3,1,2,0:T(8,128)S(1)} fusion(f32[32,128,64]{2,1,0:T(8,128)} %concatenate.64, f32[32]{0:T(128)S(1)} %add_rsqrt_fusion, f32[1,128,128]{1,2,0:T(8,128)S(1)} %get-tuple-element.26, f32[1,128,128]{1,2,0:T(8,128)S(1)} %get-tuple-element.27), kind=kOutput, calls=%fused_computation.21 | convolution fusion | flops 805601280 | bytes 3276928 | tf_op jit(solution)/shard_map/sfa,cab->cfsb/dot_general | solution.py:86
  145.0 0.2 fusion.103
  145.2 3.6 %fusion.7 = f32[32,128,128]{1,2,0:T(8,128)} fusion(f32[32,128,64]{1,2,0:T(8,128)S(1)} %get-tuple-element.12, f32[32,128,64]{1,2,0:T(8,128)S(1)} %get-tuple-element.11, f32[32,128,128]{1,2,0:T(8,128)S(1)} %bitcast.94, f32[128,128]{0,1:T(8,128)S(1)} %get-tuple-element.18, f32[128,128]{0,1:T(8,128)S(1)} %pad_maximum_fusion.7, ...), kind=kOutput, calls=%fused_computation.12 | convolution fusion | flops 807452672 | bytes 6471680 | tf_op jit(solution)/shard_map/cfk,kl->cfl/dot_general | solution.py:89
  148.8 13.1 %all-to-all-done = f32[32,32,128]{2,1,0:T(8,128)} async-done(((f32[32,32,128]{2,1,0:T(8,128)}), f32[32,32,128]{2,1,0:T(8,128)}, u32[]{:S(2)}, u32[]{:S(2)}) %all-to-all-start) | async-done | bytes 524320 | tf_op jit(solution)/shard_map/all_to_all | solution.py:131
  161.9 2.1 copy.38
  164.1 1.2 reshape.135
  165.3 1.9 fusion.25
  167.2 0.2 fusion.102
  167.4 2.3 %fusion.2 = f32[32,128,128]{1,2,0:T(8,128)S(1)} fusion(f32[32,128,64]{1,2,0:T(8,128)S(1)} %get-tuple-element.10, f32[32,128,64]{1,2,0:T(8,128)S(1)} %get-tuple-element.9, f32[32,128,128]{1,2,0:T(8,128)S(1)} %bitcast.92, f32[128,128]{0,1:T(8,128)S(1)} %get-tuple-element.18, f32[128,128]{0,1:T(8,128)S(1)} %pad_maximum_fusion.7, ...), kind=kOutput, calls=%fused_computation.7 | convolution fusion | flops 807452672 | bytes 6471680 | tf_op jit(solution)/shard_map/cfk,kl->cfl/dot_general | solution.py:89
  169.7 0.7 multiply_subtract_fusion
  170.4 2.0 fusion.11
  172.4 0.2 fusion.101
  172.7 0.6 copy-done.3
  173.3 0.5 fusion.15
  173.8 0.2 copy-done.4
  174.0 1.8 fusion.24
  175.8 1.3 copy.45
  177.2 1.4 reshape_reshape.6
  178.6 0.0 copy-start.10
  178.6 0.3 copy.46
  178.9 4.2 %all_to_all.26 = f32[16,2,32,128]{3,2,0,1:T(8,128)S(1)} all-to-all(f32[16,2,32,128]{3,2,0,1:T(8,128)S(1)} %copy.46), channel_id=1, replica_groups=mesh['grp'=2,'row'=16,'col_0'=16,'col_1'=2] {'col_1'}, dimensions={1} | all-to-all | bytes 1048576 | tf_op jit(solution)/shard_map/all_to_all | solution.py:43
  183.1 34.9 %all_to_all.27 = f32[16,2,32,128]{3,2,1,0:T(8,128)S(1)} all-to-all(f32[16,2,32,128]{3,2,1,0:T(8,128)S(1)} %copy.47), channel_id=1, replica_groups=mesh['grp'=2,'row'=16,'col_0'=16,'col_1'=2] {'col_0'}, dimensions={0} | all-to-all | bytes 1048576 | tf_op jit(solution)/shard_map/all_to_all | solution.py:43
  218.0 0.2 fusion.38
  218.2 1.5 fusion
  (29 shorter events, 0.2 us)
Async XLA Ops:
  0.0 33.4 %copy-start = (f32[128,1024]{1,0:T(8,128)S(1)}, f32[128,1024]{1,0:T(8,128)}, u32[]{:S(2)}) copy-start(f32[128,1024]{1,0:T(8,128)} %param.22) | copy-start | bytes 1572868
  3.5 8.8 %copy-start.6 = (f32[33,128]{1,0:T(8,128)S(1)}, f32[33,128]{1,0:T(8,128)}, u32[]{:S(2)}) copy-start(f32[33,128]{1,0:T(8,128)} %param.19) | copy-start | bytes 50692
  4.2 36.2 %collective-permute-start = (bf16[3,1,1024]{2,0,1:T(4,128)(2,1)S(1)}, bf16[3,1,1024]{2,0,1:T(4,128)(2,1)S(1)}, u32[]{:S(2)}, u32[]{:S(2)}) collective-permute-start(bf16[3,1,1024]{2,0,1:T(4,128)(2,1)S(1)} %copy.34), channel_id=1, source_target_pairs={{0,1},{1,2},{2,3},{3,4},{4,5},{5,6},{6,7},{7,8},{8,9},{9,10},{10,1... | collective-permute-start | bytes 18440 | tf_op jit(solution)/shard_map/ppermute | solution.py:22
  6.2 17.0 %copy-start.5 = (f32[128,128]{1,0:T(8,128)S(1)}, f32[128,128]{1,0:T(8,128)}, u32[]{:S(2)}) copy-start(f32[128,128]{1,0:T(8,128)} %param.20) | copy-start | bytes 196612
  6.6 34.3 %collective-permute-start.1 = (bf16[3,1,1024]{2,0,1:T(4,128)(2,1)S(1)}, bf16[3,1,1024]{2,0,1:T(4,128)(2,1)}, u32[]{:S(2)}, u32[]{:S(2)}) collective-permute-start(bf16[3,1,1024]{2,0,1:T(4,128)(2,1)S(1)} %copy.35), channel_id=1, source_target_pairs={{1,0},{2,1},{3,2},{4,3},{5,4},{6,5},{7,6},{8,7},{9,8},{10,9},{11,1... | collective-permute-start | bytes 18440 | tf_op jit(solution)/shard_map/ppermute | solution.py:23
  35.8 4.3 %copy-start.7 = (f32[3,1024]{1,0:T(4,128)S(1)}, f32[3,1024]{1,0:T(4,128)}, u32[]{:S(2)}) copy-start(f32[3,1024]{1,0:T(4,128)} %param.18) | copy-start | bytes 36868
  35.8 4.3 %copy-start.8 = (f32[3,1024]{1,0:T(4,128)S(1)}, f32[3,1024]{1,0:T(4,128)}, u32[]{:S(2)}) copy-start(f32[3,1024]{1,0:T(4,128)} %param.17) | copy-start | bytes 36868
  35.8 4.3 %copy-start.9 = (f32[3,1024]{1,0:T(4,128)S(1)}, f32[3,1024]{1,0:T(4,128)}, u32[]{:S(2)}) copy-start(f32[3,1024]{1,0:T(4,128)} %param.16) | copy-start | bytes 36868
  46.0 115.9 %all-to-all-start = ((f32[32,32,128]{2,1,0:T(8,128)}), f32[32,32,128]{2,1,0:T(8,128)}, u32[]{:S(2)}, u32[]{:S(2)}) async-start(f32[32,32,128]{2,1,0:T(8,128)} %bitcast.5), calls=%async_computation | async-start | bytes 1048576 | tf_op jit(solution)/shard_map/all_to_all | solution.py:131
  167.4 2.3 %copy-start.1 = (f32[32,128,128]{1,2,0:T(8,128)S(1)}, f32[32,128,128]{1,2,0:T(8,128)}, u32[]{:S(2)}) copy-start(f32[32,128,128]{1,2,0:T(8,128)} %fusion.7) | copy-start | bytes 6291460
  172.4 0.8 copy-start.3
  173.3 0.8 copy-start.4
  178.6 39.4 %copy-start.10 = (f32[1024]{0:T(1024)S(1)}, f32[1024]{0:T(1024)}, u32[]{:S(2)}) copy-start(f32[1024]{0:T(1024)} %param.24) | copy-start | bytes 12292
  183.1 35.1 %copy-start.2 = (bf16[1024,2048]{1,0:T(8,128)(2,1)S(1)}, bf16[1024,2048]{1,0:T(8,128)(2,1)}, u32[]{:S(2)}) copy-start(bf16[1024,2048]{1,0:T(8,128)(2,1)} %param.25) | copy-start | bytes 12582916
where the time goes:
time: 221 us; the launch traced here: 220 us
  starting transfers between devices  89.3 us (40%)
  matrix products  44.8 us (20%)
  blocking collectives  39 us (18%)
  local copies, waits for them, and re-layouts  21.3 us (10%)
  waiting for transfers between devices  13.1 us (6%)
  other arithmetic  11.8 us (5%)
    all_to_all x1, starting transfers between devices, body(): lax.all_to_all(product.T, COL, split_axis=0, concat_axis=1, tiled=True)  83.7 us
    all_to_all x2, blocking collectives, moved_by_axis(): result = lax.all_to_all(result, axes[k], k, k, tiled=True)  39 us
    all_to_all x1, waiting for transfers between devices, body(): lax.all_to_all(product.T, COL, split_axis=0, concat_axis=1, tiled=True)  13.1 us
    dot_general x1, matrix products, filter_hidden(): hidden = jnp.sin(jnp.dot(features, filter_first, precision=highest))  10.9 us
    dot_general x1, matrix products, filter_hidden(): hidden = jnp.sin(jnp.dot(hidden, filter_second, precision=highest))  9.4 us
    unnamed x29, local copies, waits for them, and re-layouts  7.7 us
    dot_general x2, matrix products, forward(): first = jnp.einsum('sfa,cab->cfsb', first_table, values, precision=highest)  7.08 us
    dot_general x2, matrix products, side_values(): values = jnp.einsum('pf,fh->hp', hidden, side_weight, precision=highest)  6.23 us
  transfers between devices with their start and end apart: 3, of which 1 were waited for; matrix products, arithmetic and copies ran while one was open for 23% of the time, Pallas kernels for 0%

commit v1 on v0

v1 whole, which is shorter than its diff:
```python
import functools
import math

import jax
import jax.numpy as jnp
import numpy as np
from jax import lax
from jax.experimental import pallas as pl
from jax.experimental.pallas import tpu as pltpu
from jax.sharding import PartitionSpec as P

COL = "col"
F32 = jnp.float32
BF16 = jnp.bfloat16

TWO_PI_HEAD = np.float32(np.round(2.0 * math.pi * 2**14) / 2**14)
TWO_PI_TAIL = np.float32(2.0 * math.pi - float(TWO_PI_HEAD))


def sine_coefficients():
    nodes = np.cos((np.arange(4000) + 0.5) * math.pi / 8000) * math.pi * 1.0001
    basis = np.stack([nodes ** (2 * j + 1) for j in range(7)], axis=1)
    return [float(v) for v in np.linalg.lstsq(basis, np.sin(nodes), rcond=None)[0]]


SINE = sine_coefficients()


def sine(x):
    turns = jnp.floor(x * np.float32(0.5 / math.pi) + 0.5)
    r = (x - turns * TWO_PI_HEAD) - turns * TWO_PI_TAIL
    z = r * r
    total = np.float32(SINE[6]) * z + np.float32(SINE[5])
    for j in (4, 3, 2, 1, 0):
        total = total * z + np.float32(SINE[j])
    return total * r


def halves(x):
    high = x.astype(BF16)
    return high, (x - high.astype(F32)).astype(BF16)


def np_halves(x):
    high = np.asarray(x, np.float32).astype(BF16)
    return high, (np.asarray(x, np.float32) - high.astype(np.float32)).astype(BF16)


def dot(a, b):
    return jnp.dot(a, b, preferred_element_type=F32)


def tables(blocks, width):
    span = 2 * blocks * width
    freq = np.arange(blocks) + 0.5
    first = 2.0 * math.pi * np.outer(freq, np.arange(blocks)) / (2 * blocks)
    t1 = np.concatenate([np.cos(first), -np.sin(first)], axis=0)
    t3 = np.concatenate([np.cos(first).T, -np.sin(first).T], axis=1) * (2.0 / span)
    twist = 2.0 * math.pi * np.outer(freq, np.arange(width)) / span
    second = 2.0 * math.pi * (np.outer(np.arange(width), np.arange(width)) % width) / width
    c, s = np.cos(second), np.sin(second)
    ahead = np.block([[c, -s], [s, c]])
    back = np.block([[c, s], [-s, c]])
    mirror = ahead * np.where(np.arange(2 * width) < width, 1.0, -1.0)
    t1h, t1l = np_halves(t1)
    t3h, t3l = np_halves(t3)
    return {
        "data_first": np.concatenate([t1h, t1l], axis=1),
        "kernel_first": np.concatenate([t1h, t1h, t1l], axis=1),
        "last": np.concatenate([t3h, t3h, t3l], axis=1),
        "twist": np.stack([np.cos(twist), np.sin(twist)]).astype(np.float32),
        "ahead": np.stack(np_halves(ahead)),
        "both": np.stack(np_halves(np.concatenate([ahead, mirror], axis=0))),
        "back": np.stack(np_halves(back)),
    }


def short(x, before, after, taps):
    rows = lax.broadcasted_iota(jnp.int32, x.shape, 0)
    size = x.shape[0]
    up = jnp.where(rows == 0, before, pltpu.roll(x, 1, 0))
    down = jnp.where(rows == size - 1, after, pltpu.roll(x, size - 1, 0))
    return taps[0:1] * up + taps[1:2] * x + taps[2:3] * down


def product_kernel(mult, value, before, after, taps_mult, taps_value, out):
    b, a = before[...].astype(F32), after[...].astype(F32)
    m = short(mult[...].astype(F32), b[1:2], a[1:2], taps_mult[...])
    v = short(value[...].astype(F32), b[2:3], a[2:3], taps_value[...])
    out[...] = (v * m).T.astype(BF16)


def gate_kernel(gate, mult, value, before, after, taps_gate, taps_mult, taps_value, skip, gate_out, skip_out):
    b, a = before[...].astype(F32), after[...].astype(F32)
    g = short(gate[...].astype(F32), b[0:1], a[0:1], taps_gate[...])
    m = short(mult[...].astype(F32), b[1:2], a[1:2], taps_mult[...])
    v = short(value[...].astype(F32), b[2:3], a[2:3], taps_value[...])
    gate_out[...] = g.T
    skip_out[...] = (skip[...] * (v * m)).T


def filter_kernel(
    first, second, sides, decay, kernel_first, twist, both, out, stage, left_high, left_low, *, seq_len, width, chunk
):
    hidden = second.shape[0]
    bands = (first.shape[0] - 1) // 2
    group = decay.shape[0] // 2
    blocks = seq_len // width
    padded = 2 * bands + 8
    w1 = jnp.concatenate(
        [first[1 : 1 + 2 * bands, :], first[0:1, :], jnp.zeros((padded - 2 * bands - 1, hidden), F32)], axis=0
    )
    w1h, w1l = halves(w1)
    w1s = jnp.concatenate(
        [w1h.astype(F32), w1h.astype(F32), w1l.astype(F32), jnp.zeros((128 - 3 * padded, hidden), F32)], axis=0
    ).T.astype(BF16)
    w2h, w2l = halves(second[...].T)
    w2s = jnp.concatenate([w2h, w2h, w2l], axis=1)
    w3h, w3l = halves(sides[...].T)
    w3s = jnp.concatenate([w3h, w3h, w3l], axis=1)
    row = lax.broadcasted_iota(jnp.int32, (2 * bands, chunk), 0)
    band_at = jnp.where(row < bands, row, row - bands).astype(F32)
    band = np.float32(0.0001) + band_at * np.float32((bands - 1 - 0.0001) / (bands - 1))
    band = jnp.where(row < bands, band, -band)
    offset = jnp.where(row < bands, np.float32(0.5 * math.pi), np.float32(0.0))
    head_row = lax.broadcasted_iota(jnp.int32, (8, chunk), 0)
    rates = decay[...]

    def step(i, total):
        at = i * chunk
        position = (lax.broadcasted_iota(jnp.int32, (1, chunk), 1) + at).astype(F32)
        tau = position / np.float32(seq_len - 1)
        omega = position * np.float32(2.0 * math.pi / seq_len)
        trig = sine(omega * band + offset)
        feats = jnp.concatenate([trig, jnp.where(head_row == 0, tau, 0.0)], axis=0)
        fh = feats.astype(BF16).astype(F32)
        fs = jnp.concatenate(
            [fh, feats - fh, fh, jnp.zeros((128 - 3 * padded, chunk), F32)], axis=0
        ).astype(BF16)
        h1h, h1l = halves(sine(dot(w1s, fs)))
        h2h, h2l = halves(sine(dot(w2s, jnp.concatenate([h1h, h1l, h1h], axis=0))))
        values = dot(w3s, jnp.concatenate([h2h, h2l, h2h], axis=0))
        values = values * jnp.exp(-rates * tau)
        side_row = lax.broadcasted_iota(jnp.int32, values.shape, 0)
        values = jnp.where((side_row >= group) & (position < 0.5), 0.0, values)
        for j in range(chunk // width):
            part = values[:, j * width : (j + 1) * width]
            total = total + part * part
            start = pl.multiple_of((i * (chunk // width) + j) * 2 * group, 2 * group)
            stage[pl.ds(start, 2 * group), :] = part
        return total

    total = lax.fori_loop(0, seq_len // chunk, step, jnp.zeros((2 * group, width), F32))
    power = jnp.sum(total, axis=1, keepdims=True)
    scale = lax.rsqrt(power[:group] + power[group:] + np.float32(1e-06))
    cos, sin = twist[0], twist[1]
    cos2, sin2 = jnp.concatenate([cos, cos], axis=1), jnp.concatenate([sin, sin], axis=1)
    for c in range(group):
        x = jnp.concatenate(
            [stage[pl.ds(c, blocks, stride=2 * group), :], stage[pl.ds(group + c, blocks, stride=2 * group), :]], axis=1
        )
        xh, xl = halves(x * scale[c : c + 1, :])
        z = dot(kernel_first[...], jnp.concatenate([xh, xl, xh], axis=0))
        re, im = z[:blocks], z[blocks:]
        re, im = re * cos2 + im * sin2, im * cos2 - re * sin2
        left = jnp.concatenate([re[:, :width], im[:, :width], re[:, width:], im[:, width:]], axis=1)
        high, low = halves(left)
        left_high[c * blocks : (c + 1) * blocks, :] = high
        left_low[c * blocks : (c + 1) * blocks, :] = low
    out[...] = dot(left_high[...], both[0]) + dot(left_low[...], both[0]) + dot(left_high[...], both[1])


def conv_kernel(data, spec, data_first, twist, ahead, back, last, out, stage, left_high, left_low, *, group):
    width = data.shape[1]
    blocks = data.shape[0] // group
    cos, sin = twist[0], twist[1]
    stage[...] = data[...].astype(F32)
    for c in range(group):
        x = stage[pl.ds(c, blocks, stride=group), :].astype(BF16)
        z = dot(data_first[...], jnp.concatenate([x, x], axis=0))
        re, im = z[:blocks], z[blocks:]
        left = jnp.concatenate([re * cos + im * sin, im * cos - re * sin], axis=1)
        high, low = halves(left)
        left_high[c * blocks : (c + 1) * blocks, :] = high
        left_low[c * blocks : (c + 1) * blocks, :] = low
    s = dot(left_high[...], ahead[0]) + dot(left_low[...], ahead[0]) + dot(left_high[...], ahead[1])
    sr, si = s[:, :width], s[:, width:]
    kr, ki = spec[:, :width], spec[:, width:]
    high, low = halves(jnp.concatenate([sr * kr - si * ki, sr * ki + si * kr], axis=1))
    v = dot(high, back[0]) + dot(low, back[0]) + dot(high, back[1])
    for c in range(group):
        vr = v[c * blocks : (c + 1) * blocks, :width]
        vi = v[c * blocks : (c + 1) * blocks, width:]
        high, low = halves(jnp.concatenate([vr * cos - vi * sin, vi * cos + vr * sin], axis=0))
        stage[pl.ds(c, blocks, stride=group), :] = dot(last[...], jnp.concatenate([high, low, high], axis=0))
    out[...] = stage[...].astype(BF16)


def body(
    gate_in,
    mult_in,
    value_in,
    taps_gate,
    taps_mult,
    taps_value,
    filter_first,
    filter_second,
    filter_ahead,
    filter_behind,
    filter_decay,
    skip_gain,
    out_weight,
):
    cols = lax.axis_size(COL)
    col = lax.axis_index(COL)
    width, channels = gate_in.shape[1:]
    seq_len = width * cols
    group = channels // cols
    gate, mult, value = gate_in[0], mult_in[0], value_in[0]
    t = tables(cols, width)

    up = [(i, i + 1) for i in range(cols - 1)]
    down = [(j, i) for i, j in up]
    before = lax.ppermute(jnp.concatenate([gate[-1:], mult[-1:], value[-1:]]), COL, up)
    after = lax.ppermute(jnp.concatenate([gate[:1], mult[:1], value[:1]]), COL, down)
    product = pl.pallas_call(product_kernel, out_shape=jax.ShapeDtypeStruct((channels, width), BF16), name="product")(
        mult, value, before, after, taps_mult, taps_value
    )
    spread = lax.all_to_all(product.reshape(cols, group, width), COL, 0, 0, tiled=True)

    first = col * group
    sides = jnp.concatenate(
        [lax.dynamic_slice_in_dim(w, first, group, 1) for w in (filter_ahead, filter_behind)], axis=1
    )
    rates = lax.dynamic_slice_in_dim(filter_decay, first, group)
    rates = jnp.concatenate([rates, rates])[:, None]
    spec = pl.pallas_call(
        functools.partial(filter_kernel, seq_len=seq_len, width=width, chunk=4 * width),
        out_shape=jax.ShapeDtypeStruct((group * cols, 2 * width), F32),
        scratch_shapes=[
            pltpu.VMEM((2 * group * cols, width), F32),
            pltpu.VMEM((group * cols, 4 * width), BF16),
            pltpu.VMEM((group * cols, 4 * width), BF16),
        ],
        name="filter",
    )(filter_first, filter_second, sides, rates, t["kernel_first"], t["twist"], t["both"])
    gate_part, skip_part = pl.pallas_call(
        gate_kernel,
        out_shape=[jax.ShapeDtypeStruct((channels, width), F32)] * 2,
        name="gate",
    )(gate, mult, value, before, after, taps_gate, taps_mult, taps_value, skip_gain[None])

    convolved = pl.pallas_call(
        functools.partial(conv_kernel, group=group),
        out_shape=jax.ShapeDtypeStruct((channels, width), BF16),
        scratch_shapes=[
            pltpu.VMEM((channels, width), F32),
            pltpu.VMEM((channels, 2 * width), BF16),
            pltpu.VMEM((channels, 2 * width), BF16),
        ],
        name="conv",
    )(spread.reshape(channels, width), spec, t["data_first"], t["twist"], t["ahead"], t["back"], t["last"])
    returned = lax.all_to_all(convolved.reshape(cols, group, width), COL, 0, 0, tiled=True)
    gated = ((returned.reshape(channels, width).astype(F32) + skip_part) * gate_part).astype(BF16)
    mixed = lax.dot_general(gated, out_weight, (((0,), (0,)), ((), ())), preferred_element_type=F32)
    return mixed.astype(BF16)[None]


def solution(mesh):
    tokens = P(("grp", "row"), COL, None)
    in_specs = (tokens,) * 3 + (P(),) * 10
    return jax.shard_map(body, mesh=mesh, in_specs=in_specs, out_specs=tokens, check_vma=False)
```

time: 221 us -> 156 us (0.71)
  the two profiles are of different devices: /device:TPU:12 before, /device:TPU:5 now
where the time goes in v1:
time: 156 us; the launch traced here: 155 us
  starting transfers between devices  97.1 us (62%)
  waiting for transfers between devices  26.7 us (17%)
  Pallas kernels  21.3 us (14%)
  local copies, waits for them, and re-layouts  5.26 us (3%)
  matrix products  4.06 us (3%)
    ppermute x1, starting transfers between devices, body(): lax.ppermute(jnp.concatenate([gate[:1], mult[:1], value[:1]]), COL, down)  82 us
    all_to_all x1, waiting for transfers between devices, body(): lax.all_to_all(convolved.reshape(cols, group, width), COL, 0, 0, tiled=True)  19.5 us
    pallas_call x1, Pallas kernels, body(): pl.pallas_call(functools.partial(filter_kernel, seq_len=seq_len, width=wi...  11.7 us
    all_to_all x1, waiting for transfers between devices, body(): lax.all_to_all(product.reshape(cols, group, width), COL, 0, 0, tiled=True)  6.39 us
    all_to_all x1, starting transfers between devices, body(): lax.all_to_all(convolved.reshape(cols, group, width), COL, 0, 0, tiled=True)  6.22 us
    ppermute x1, starting transfers between devices, body(): lax.ppermute(jnp.concatenate([gate[-1:], mult[-1:], value[-1:]]), COL, up)  4.76 us
    pallas_call x1, Pallas kernels, body(): pl.pallas_call(functools.partial(conv_kernel, group=group), out_shape=jax...  4.71 us
    all_to_all x1, starting transfers between devices, body(): lax.all_to_all(product.reshape(cols, group, width), COL, 0, 0, tiled=True)  4.19 us
  transfers between devices with their start and end apart: 4, of which 3 were waited for; matrix products, arithmetic and copies ran while one was open for 2% of the time, Pallas kernels for 9%

profile of v1, /device:TPU:5, one launch (start us, length us, event | category | flops | bytes accessed | tf_op | source)
XLA Modules:
  0.0 155.3 jit_solution(12631559863358768479)
XLA Ops:
  0.0 0.7 slice_bitcast_fusion.2
  0.7 0.8 slice_bitcast_fusion
  1.6 4.8 %collective-permute-start = (bf16[3,1024]{1,0:T(4,128)(2,1)S(1)}, bf16[3,1024]{1,0:T(4,128)(2,1)S(1)}, u32[]{:S(2)}, u32[]{:S(2)}) collective-permute-start(bf16[3,1024]{1,0:T(4,128)(2,1)S(1)} %pad_maximum_fusion.1), channel_id=1, source_target_pairs={{0,1},{1,2},{2,3},{3,4},{4,5},{5,6},{6,7},{7,8},{8,9},{9,10},{10,1... | collective-permute-start | bytes 18440 | tf_op jit(solution)/shard_map/ppermute | solution.py:224
  6.4 82.0 %collective-permute-start.1 = (bf16[3,1024]{1,0:T(4,128)(2,1)S(1)}, bf16[3,1024]{1,0:T(4,128)(2,1)S(1)}, u32[]{:S(2)}, u32[]{:S(2)}) collective-permute-start(bf16[3,1024]{1,0:T(4,128)(2,1)S(1)} %pad_maximum_fusion.2), channel_id=1, source_target_pairs={{1,0},{2,1},{3,2},{4,3},{5,4},{6,5},{7,6},{8,7},{9,8},{10,9},{11,1... | collective-permute-start | bytes 18440 | tf_op jit(solution)/shard_map/ppermute | solution.py:225
  88.3 0.0 collective-permute-done.before
  88.3 0.0 copy-start.1
  88.3 0.8 collective-permute-done.1.after
  89.1 0.0 copy-start.2
  89.1 0.0 copy-done.1
  89.1 0.6 copy-done.2
  89.7 2.3 %product.1 = bf16[1024,128]{1,0:T(8,128)(2,1)} custom-call(bf16[128,1024]{1,0:T(8,128)(2,1)} %bitcast.26, bf16[128,1024]{1,0:T(8,128)(2,1)} %bitcast.28, bf16[3,1024]{1,0:T(4,128)(2,1)} %copy-done.1, bf16[3,1024]{1,0:T(4,128)(2,1)} %copy-done.2, f32[3,1024]{1,0:T(4,128)} %taps_mult.3, f32[3,1024]{1,0:T(4,128)} %taps_value.3), custom_call_target="tpu_custom_call" | custom-call | tf_op jit(solution)/shard_map/product/pallas_call | solution.py:226
  92.0 4.2 %all-to-all-start = ((bf16[32,32,128]{2,1,0:T(8,128)(2,1)}), bf16[32,32,128]{2,1,0:T(8,128)(2,1)S(1)}, u32[]{:S(2)}, u32[]{:S(2)}) async-start(bf16[32,32,128]{2,1,0:T(8,128)(2,1)} %bitcast.31), calls=%async_computation | async-start | bytes 524288 | tf_op jit(solution)/shard_map/all_to_all | solution.py:229
  96.2 0.8 dynamic_slice.11
  97.0 0.1 maximum_bitcast_fusion
  97.0 0.7 copy.21.decay
  97.7 1.0 constant_dynamic-slice_fusion
  98.7 0.7 pad_maximum_fusion.sides
  99.4 11.7 %filter.1.spec = f32[1024,256]{1,0:T(8,128)} custom-call(f32[33,128]{1,0:T(8,128)} %first.1, f32[128,128]{1,0:T(8,128)} %second.1, f32[128,64]{1,0:T(8,128)} %pad_maximum_fusion.sides, f32[64,1]{1,0:T(8,128)} %copy.21.decay, bf16[64,96]{1,0:T(8,128)(2,1)} %constant.24.clone.kernel_first, f32[2,32,128]{2,1,0:T(8,128)} %constant.25.clone.twist, ...), custom_call_target="tpu_custom_call" | custom-call | tf_op jit(solution)/shard_map/filter/pallas_call | solution.py:237
  111.1 6.4 %all-to-all-done = bf16[32,32,128]{2,1,0:T(8,128)(2,1)S(1)} async-done(((bf16[32,32,128]{2,1,0:T(8,128)(2,1)}), bf16[32,32,128]{2,1,0:T(8,128)(2,1)S(1)}, u32[]{:S(2)}, u32[]{:S(2)}) %all-to-all-start) | async-done | bytes 262176 | tf_op jit(solution)/shard_map/all_to_all | solution.py:229
  117.5 0.0 copy-start
  117.5 0.7 copy-done
  118.2 4.7 %conv.1 = bf16[1024,128]{1,0:T(8,128)(2,1)} custom-call(bf16[1024,128]{1,0:T(8,128)(2,1)} %bitcast.30, f32[1024,256]{1,0:T(8,128)} %filter.1.spec, bf16[64,64]{1,0:T(8,128)(2,1)} %constant.27.clone.data_first, f32[2,32,128]{2,1,0:T(8,128)} %constant.25.clone.twist, bf16[2,256,256]{2,1,0:T(8,128)(2,1)} %constant.28.clone.ahead, ...), custom_call_target="tpu_custom_call" | custom-call | tf_op jit(solution)/shard_map/conv/pallas_call | solution.py:253
  122.9 6.2 %all-to-all-start.1 = ((bf16[32,32,128]{2,1,0:T(8,128)(2,1)}), bf16[32,32,128]{2,1,0:T(8,128)(2,1)S(1)}, u32[]{:S(2)}, u32[]{:S(2)}) async-start(bf16[32,32,128]{2,1,0:T(8,128)(2,1)} %bitcast.32), calls=%async_computation.1 | async-start | bytes 524288 | tf_op jit(solution)/shard_map/all_to_all | solution.py:263
  129.2 2.6 %gate.1 = (f32[1024,128]{1,0:T(8,128)}, f32[1024,128]{1,0:T(8,128)}) custom-call(bf16[128,1024]{1,0:T(8,128)(2,1)} %bitcast.34, bf16[128,1024]{1,0:T(8,128)(2,1)} %bitcast.27, bf16[128,1024]{1,0:T(8,128)(2,1)} %bitcast.29, bf16[3,1024]{1,0:T(4,128)(2,1)} %copy-done.1, bf16[3,1024]{1,0:T(4,128)(2,1)} %copy-done.2, f32[3,1024]{1,0:T(4,128)} %taps_gate.1, ...), custom_call_target="tpu_custom_call" | custom-call | tf_op jit(solution)/shard_map/gate/pallas_call | solution.py:247
  131.8 19.5 %all-to-all-done.1 = bf16[32,32,128]{2,1,0:T(8,128)(2,1)S(1)} async-done(((bf16[32,32,128]{2,1,0:T(8,128)(2,1)}), bf16[32,32,128]{2,1,0:T(8,128)(2,1)S(1)}, u32[]{:S(2)}, u32[]{:S(2)}) %all-to-all-start.1) | async-done | bytes 262176 | tf_op jit(solution)/shard_map/all_to_all | solution.py:263
  151.3 4.1 %fusion = bf16[1,128,2048]{2,1,0:T(8,128)(2,1)} fusion(bf16[1024,2048]{1,0:T(8,128)(2,1)} %param.32, f32[1024,128]{1,0:T(8,128)} %get-tuple-element.8, f32[1024,128]{1,0:T(8,128)} %get-tuple-element.7, bf16[1024,128]{1,0:T(8,128)(2,1)S(1)} %bitcast.33), kind=kOutput, calls=%fused_computation.1 | convolution fusion | flops 537657344 | bytes 6029312 | tf_op jit(solution)/shard_map/dot_general | solution.py:265
  (2 shorter events, 0.0 us)
Async XLA Ops:
  1.6 86.8 %collective-permute-start = (bf16[3,1024]{1,0:T(4,128)(2,1)S(1)}, bf16[3,1024]{1,0:T(4,128)(2,1)S(1)}, u32[]{:S(2)}, u32[]{:S(2)}) collective-permute-start(bf16[3,1024]{1,0:T(4,128)(2,1)S(1)} %pad_maximum_fusion.1), channel_id=1, source_target_pairs={{0,1},{1,2},{2,3},{3,4},{4,5},{5,6},{6,7},{7,8},{8,9},{9,10},{10,1... | collective-permute-start | bytes 18440 | tf_op jit(solution)/shard_map/ppermute | solution.py:224
  6.4 82.8 %collective-permute-start.1 = (bf16[3,1024]{1,0:T(4,128)(2,1)S(1)}, bf16[3,1024]{1,0:T(4,128)(2,1)S(1)}, u32[]{:S(2)}, u32[]{:S(2)}) collective-permute-start(bf16[3,1024]{1,0:T(4,128)(2,1)S(1)} %pad_maximum_fusion.2), channel_id=1, source_target_pairs={{1,0},{2,1},{3,2},{4,3},{5,4},{6,5},{7,6},{8,7},{9,8},{10,9},{11,1... | collective-permute-start | bytes 18440 | tf_op jit(solution)/shard_map/ppermute | solution.py:225
  88.3 0.8 copy-start.1
  89.1 0.6 copy-start.2
  92.0 25.5 %all-to-all-start = ((bf16[32,32,128]{2,1,0:T(8,128)(2,1)}), bf16[32,32,128]{2,1,0:T(8,128)(2,1)S(1)}, u32[]{:S(2)}, u32[]{:S(2)}) async-start(bf16[32,32,128]{2,1,0:T(8,128)(2,1)} %bitcast.31), calls=%async_computation | async-start | bytes 524288 | tf_op jit(solution)/shard_map/all_to_all | solution.py:229
  117.5 0.7 copy-start
  122.9 28.3 %all-to-all-start.1 = ((bf16[32,32,128]{2,1,0:T(8,128)(2,1)}), bf16[32,32,128]{2,1,0:T(8,128)(2,1)S(1)}, u32[]{:S(2)}, u32[]{:S(2)}) async-start(bf16[32,32,128]{2,1,0:T(8,128)(2,1)} %bitcast.32), calls=%async_computation.1 | async-start | bytes 524288 | tf_op jit(solution)/shard_map/all_to_all | solution.py:263

commit v2 on v1

--- a/solution.py
+++ b/solution.py
@@ -7,9 +7,14 @@
 from jax import lax
 from jax.experimental import pallas as pl
 from jax.experimental.pallas import tpu as pltpu
+from jax.sharding import Mesh
 from jax.sharding import PartitionSpec as P
 
-COL = "col"
+CHIP = "col_chip"
+CORE = "col_core"
+COL = (CHIP, CORE)
+CORES = 2
+EDGE = 8
 F32 = jnp.float32
 BF16 = jnp.bfloat16
 
@@ -44,6 +49,14 @@
 def np_halves(x):
     high = np.asarray(x, np.float32).astype(BF16)
     return high, (np.asarray(x, np.float32) - high.astype(np.float32)).astype(BF16)
+
+
+def cost(microseconds, size):
+    return pl.CostEstimate(flops=int(microseconds * 4e8), bytes_accessed=size, transcendentals=0)
+
+
+def limit(mebibytes):
+    return pltpu.CompilerParams(vmem_limit_bytes=mebibytes * 2**20)
 
 
 def dot(a, b):
@@ -83,28 +96,67 @@
     return taps[0:1] * up + taps[1:2] * x + taps[2:3] * down
 
 
-def product_kernel(mult, value, before, after, taps_mult, taps_value, out):
-    b, a = before[...].astype(F32), after[...].astype(F32)
-    m = short(mult[...].astype(F32), b[1:2], a[1:2], taps_mult[...])
-    v = short(value[...].astype(F32), b[2:3], a[2:3], taps_value[...])
-    out[...] = (v * m).T.astype(BF16)
-
-
-def gate_kernel(gate, mult, value, before, after, taps_gate, taps_mult, taps_value, skip, gate_out, skip_out):
+def product_kernel(mult, value, taps_mult, taps_value, out):
+    m, v = mult[...].astype(F32), value[...].astype(F32)
+    zero = jnp.zeros((1, m.shape[1]), F32)
+    product = short(v, zero, zero, taps_value[...]) * short(m, zero, zero, taps_mult[...])
+    product = product.T.astype(BF16)
+    edges = jnp.concatenate([v[:2], m[:2], v[-2:], m[-2:]], axis=0).astype(BF16)
+    chips, rows, width = out.shape
+    part = (rows - EDGE) // 2
+    for k in range(chips):
+        at = 2 * part * k
+        lane = at // width * width
+        out[k, :part, :] = product[at : at + part]
+        out[k, part : part + EDGE, :] = edges[:, lane : lane + width]
+        out[k, part + EDGE :, :] = product[at + part : at + 2 * part]
+
+
+def gate_kernel(
+    gate, mult, value, before, after, taps_gate, taps_mult, taps_value, skip, gate_out, skip_out
+):
     b, a = before[...].astype(F32), after[...].astype(F32)
     g = short(gate[...].astype(F32), b[0:1], a[0:1], taps_gate[...])
     m = short(mult[...].astype(F32), b[1:2], a[1:2], taps_mult[...])
     v = short(value[...].astype(F32), b[2:3], a[2:3], taps_value[...])
-    gate_out[...] = g.T
-    skip_out[...] = (skip[...] * (v * m)).T
+    gate_out[...] = g
+    skip_out[...] = skip[...] * (v * m)
+
+
+def mix_kernel(planes, other, gate_part, skip_part, weight, out, stage):
+    core = lax.axis_index(CORE)
+    chips, rows, _ = planes.shape
+    group = rows // CORES
+    for k in range(chips):
+        near = pl.multiple_of(rows * k + core * group, group)
+        far = pl.multiple_of(rows * k + (1 - core) * group, group)
+        stage[pl.ds(near, group), :] = planes[k, pl.ds(pl.multiple_of(core * group, group), group), :].astype(F32)
+        stage[pl.ds(far, group), :] = other[k].astype(F32)
+    gated = ((stage[...].T + skip_part[...]) * gate_part[...]).astype(BF16)
+    out[...] = dot(gated, weight[...]).astype(BF16)
 
 
 def filter_kernel(
-    first, second, sides, decay, kernel_first, twist, both, out, stage, left_high, left_low, *, seq_len, width, chunk
+    *refs, seq_len, width, chunk, group
 ):
+    sources, out, copies, (own, stage, left_high, left_low, sems) = refs[:8], refs[8], refs[9:17], refs[17:]
+    moves = [pltpu.make_async_copy(a, b, sems.at[n]) for n, (a, b) in enumerate(zip(sources, copies))]
+    for move in moves:
+        move.start()
+    for move in moves:
+        move.wait()
+    first, second, ahead, behind, decay, kernel_first, twist, both = copies
     hidden = second.shape[0]
     bands = (first.shape[0] - 1) // 2
-    group = decay.shape[0] // 2
+    channel = (lax.axis_index(CHIP) * CORES + lax.axis_index(CORE)) * group
+    lane = pl.multiple_of(channel // width * width, width)
+    row_at = pl.multiple_of(channel % width, group)
+    own[0] = ahead[:, pl.ds(lane, width)].T
+    own[1] = behind[:, pl.ds(lane, width)].T
+    own[2] = jnp.broadcast_to(decay[:, pl.ds(lane, width)], (width, width)).T
+    sides = jnp.concatenate([own[0, pl.ds(row_at, group), :], own[1, pl.ds(row_at, group), :]], axis=0)
+    rates = own[2, pl.ds(row_at, group), :][:, 0:1]
+    rates = jnp.concatenate([rates, rates], axis=0)
     blocks = seq_len // width
     padded = 2 * bands + 8
     w1 = jnp.concatenate(
@@ -116,7 +168,7 @@
     ).T.astype(BF16)
     w2h, w2l = halves(second[...].T)
     w2s = jnp.concatenate([w2h, w2h, w2l], axis=1)
-    w3h, w3l = halves(sides[...].T)
+    w3h, w3l = halves(sides)
     w3s = jnp.concatenate([w3h, w3h, w3l], axis=1)
     row = lax.broadcasted_iota(jnp.int32, (2 * bands, chunk), 0)
     band_at = jnp.where(row < bands, row, row - bands).astype(F32)
@@ -124,7 +176,6 @@
     band = jnp.where(row < bands, band, -band)
     offset = jnp.where(row < bands, np.float32(0.5 * math.pi), np.float32(0.0))
     head_row = lax.broadcasted_iota(jnp.int32, (8, chunk), 0)
-    rates = decay[...]
 
     def step(i, total):
         at = i * chunk
@@ -170,13 +221,50 @@
     out[...] = dot(left_high[...], both[0]) + dot(left_low[...], both[0]) + dot(left_high[...], both[1])
 
 
-def conv_kernel(data, spec, data_first, twist, ahead, back, last, out, stage, left_high, left_low, *, group):
-    width = data.shape[1]
-    blocks = data.shape[0] // group
+def conv_kernel(
+    plane, partner, taps_mult, taps_value, spec, data_first, twist, ahead, back, last, out, stage, left_high, left_low,
+    *, group
+):
+    chips, rows, width = partner.shape
+    blocks = chips * CORES
+    chip, core = lax.axis_index(CHIP), lax.axis_index(CORE)
+    pitch = group + 2 * EDGE
+    base = pl.multiple_of(EDGE * (1 - core), EDGE)
+    own_at = pl.multiple_of(core * group, group)
+    for k in range(chips):
+        near = pl.multiple_of((CORES * k + core) * pitch + base, EDGE)
+        far = pl.multiple_of((CORES * k + 1 - core) * pitch + base, EDGE)
+        stage[pl.ds(near, rows), :] = plane[k, pl.ds(own_at, rows), :].astype(F32)
+        stage[pl.ds(far, rows), :] = partner[k].astype(F32)
+
+    channel = (chip * CORES + core) * group
+    lane = pl.multiple_of(channel // width * width, width)
+    tm, tv = taps_mult[:, pl.ds(lane, width)], taps_value[:, pl.ds(lane, width)]
+    edge_at = (group + EDGE) * (1 - core)
+    v0, v1, m0, m1, v2, v3, m2, m3 = [stage[pl.ds(edge_at + q, blocks, stride=pitch), :] for q in range(EDGE)]
+    row = lax.broadcasted_iota(jnp.int32, (blocks, width), 0)
+    column = lax.broadcasted_iota(jnp.int32, (blocks, width), 1)
+
+    def head(t, previous, x, following):
+        return t[0:1] * jnp.where(row == 0, 0.0, pltpu.roll(previous, 1, 0)) + t[1:2] * x + t[2:3] * following
+
+    def tail(t, previous, x, following):
+        after = jnp.where(row == blocks - 1, 0.0, pltpu.roll(following, blocks - 1, 0))
+        return t[0:1] * previous + t[1:2] * x + t[2:3] * after
+
+    heads = head(tv, v3, v0, v1) * head(tm, m3, m0, m1)
+    tails = tail(tv, v2, v3, v0) * tail(tm, m2, m3, m0)
+    shift = width - channel % width
+    heads = pltpu.roll(heads, shift, 1)
+    tails = pltpu.roll(tails, shift + width - 1, 1)
+    odd = column % 2 == 1
+    edges = (jnp.where(odd, tails, heads), jnp.where(odd, heads, tails))
+    border = (column == 0) | (column == width - 1)
+
     cos, sin = twist[0], twist[1]
-    stage[...] = data[...].astype(F32)
     for c in range(group):
-        x = stage[pl.ds(c, blocks, stride=group), :].astype(BF16)
+        x = stage[pl.ds(EDGE + c, blocks, stride=pitch), :]
+        x = jnp.where(border, pltpu.roll(edges[c % 2], (width - c) % width, 1), x).astype(BF16)
         z = dot(data_first[...], jnp.concatenate([x, x], axis=0))
         re, im = z[:blocks], z[blocks:]
         left = jnp.concatenate([re * cos + im * sin, im * cos - re * sin], axis=1)
@@ -193,7 +281,7 @@
         vi = v[c * blocks : (c + 1) * blocks, width:]
         high, low = halves(jnp.concatenate([vr * cos - vi * sin, vi * cos + vr * sin], axis=0))
         stage[pl.ds(c, blocks, stride=group), :] = dot(last[...], jnp.concatenate([high, low, high], axis=0))
-    out[...] = stage[...].astype(BF16)
+    out[...] = stage[: blocks * group, :].astype(BF16)
 
 
 def body(
@@ -211,62 +299,90 @@
     skip_gain,
     out_weight,
 ):
-    cols = lax.axis_size(COL)
-    col = lax.axis_index(COL)
+    chips, core = lax.axis_size(CHIP), lax.axis_index(CORE)
+    cols = chips * CORES
     width, channels = gate_in.shape[1:]
     seq_len = width * cols
     group = channels // cols
     gate, mult, value = gate_in[0], mult_in[0], value_in[0]
     t = tables(cols, width)
-
+    swap = [(i, i + 1 - 2 * (i % CORES)) for i in range(cols)]
     up = [(i, i + 1) for i in range(cols - 1)]
     down = [(j, i) for i, j in up]
-    before = lax.ppermute(jnp.concatenate([gate[-1:], mult[-1:], value[-1:]]), COL, up)
-    after = lax.ppermute(jnp.concatenate([gate[:1], mult[:1], value[:1]]), COL, down)
-    product = pl.pallas_call(product_kernel, out_shape=jax.ShapeDtypeStruct((channels, width), BF16), name="product")(
-        mult, value, before, after, taps_mult, taps_value
+
+    rows = CORES * group + EDGE
+    product = pl.pallas_call(
+        product_kernel,
+        out_shape=jax.ShapeDtypeStruct((chips, rows, width), BF16),
+        compiler_params=pltpu.CompilerParams(vmem_limit_bytes=67_000_000),
+        name="product",
+    )(mult, value, taps_mult, taps_value)
+    plane = lax.all_to_all(product, CHIP, 0, 0, tiled=True)
+    filter_args = (
+        filter_first, filter_second, filter_ahead, filter_behind, filter_decay[None], t["kernel_first"], t["twist"], t["both"]
     )
-    spread = lax.all_to_all(product.reshape(cols, group, width), COL, 0, 0, tiled=True)
-
-    first = col * group
-    sides = jnp.concatenate(
-        [lax.dynamic_slice_in_dim(w, first, group, 1) for w in (filter_ahead, filter_behind)], axis=1
-    )
-    rates = lax.dynamic_slice_in_dim(filter_decay, first, group)
-    rates = jnp.concatenate([rates, rates])[:, None]
     spec = pl.pallas_call(
-        functools.partial(filter_kernel, seq_len=seq_len, width=width, chunk=4 * width),
+        functools.partial(filter_kernel, seq_len=seq_len, width=width, chunk=4 * width, group=group),
+        in_specs=[pl.BlockSpec(memory_space=pltpu.HBM)] * len(filter_args),
         out_shape=jax.ShapeDtypeStruct((group * cols, 2 * width), F32),
-        scratch_shapes=[
+        scratch_shapes=[pltpu.VMEM(x.shape, x.dtype) for x in filter_args]
+        + [
+            pltpu.VMEM((3, width, width), F32),
             pltpu.VMEM((2 * group * cols, width), F32),
             pltpu.VMEM((group * cols, 4 * width), BF16),
             pltpu.VMEM((group * cols, 4 * width), BF16),
+            pltpu.SemaphoreType.DMA((len(filter_args),)),
         ],
+        compiler_params=limit(16),
+        cost_estimate=cost(10, 2**22),
         name="filter",
-    )(filter_first, filter_second, sides, rates, t["kernel_first"], t["twist"], t["both"])
-    gate_part, skip_part = pl.pallas_call(
-        gate_kernel,
-        out_shape=[jax.ShapeDtypeStruct((channels, width), F32)] * 2,
-        name="gate",
-    )(gate, mult, value, before, after, taps_gate, taps_mult, taps_value, skip_gain[None])
+    )(*filter_args)
+    plane, spec = lax.optimization_barrier((plane, spec))
+    partner = lax.ppermute(lax.dynamic_slice_in_dim(plane, (1 - core) * group, group + EDGE, 1), COL, swap)
 
     convolved = pl.pallas_call(
         functools.partial(conv_kernel, group=group),
         out_shape=jax.ShapeDtypeStruct((channels, width), BF16),
         scratch_shapes=[
-            pltpu.VMEM((channels, width), F32),
+            pltpu.VMEM((cols * (group + 2 * EDGE), width), F32),
             pltpu.VMEM((channels, 2 * width), BF16),
             pltpu.VMEM((channels, 2 * width), BF16),
         ],
+        compiler_params=limit(16),
+        cost_estimate=cost(3, 2**21),
         name="conv",
-    )(spread.reshape(channels, width), spec, t["data_first"], t["twist"], t["ahead"], t["back"], t["last"])
-    returned = lax.all_to_all(convolved.reshape(cols, group, width), COL, 0, 0, tiled=True)
-    gated = ((returned.reshape(channels, width).astype(F32) + skip_part) * gate_part).astype(BF16)
-    mixed = lax.dot_general(gated, out_weight, (((0,), (0,)), ((), ())), preferred_element_type=F32)
-    return mixed.astype(BF16)[None]
+    )(plane, partner, taps_mult, taps_value, spec, t["data_first"], t["twist"], t["ahead"], t["back"], t["last"])
+
+    convolved, gate, mult, value = lax.optimization_barrier((convolved, gate, mult, value))
+    planes = lax.all_to_all(convolved.reshape(chips, CORES * group, width), CHIP, 0, 0, tiled=True)
+    before = lax.ppermute(jnp.concatenate([gate[-1:], mult[-1:], value[-1:]]), COL, up)
+    after = lax.ppermute(jnp.concatenate([gate[:1], mult[:1], value[:1]]), COL, down)
+    gate_part, skip_part = pl.pallas_call(
+        gate_kernel,
+        out_shape=[jax.ShapeDtypeStruct((width, channels), F32)] * 2,
+        compiler_params=limit(12),
+        cost_estimate=cost(20, 2**21),
+        name="gate",
+    )(gate, mult, value, before, after, taps_gate, taps_mult, taps_value, skip_gain[None])
+    planes, gate_part, skip_part = lax.optimization_barrier((planes, gate_part, skip_part))
+    theirs = lax.dynamic_slice_in_dim(planes, (1 - core) * group, group, 1)
+    other = lax.ppermute(theirs, COL, swap)
+    mixed = pl.pallas_call(
+        mix_kernel,
+        out_shape=jax.ShapeDtypeStruct((width, out_weight.shape[1]), BF16),
+        scratch_shapes=[pltpu.VMEM((channels, width), F32)],
+        compiler_params=limit(12),
+        cost_estimate=cost(2, 2**22),
+        name="mix",
+    )(planes, other, gate_part, skip_part, out_weight)
+    return mixed[None]
 
 
 def solution(mesh):
+    shape = mesh.shape
+    split = Mesh(
+        mesh.devices.reshape(shape["grp"], shape["row"], shape["col"] // CORES, CORES), ("grp", "row", CHIP, CORE)
+    )
     tokens = P(("grp", "row"), COL, None)
     in_specs = (tokens,) * 3 + (P(),) * 10
-    return jax.shard_map(body, mesh=mesh, in_specs=in_specs, out_specs=tokens, check_vma=False)
+    return jax.shard_map(body, mesh=split, in_specs=in_specs, out_specs=tokens, check_vma=False)

time: 156 us -> 152 us (0.974)
  waiting for transfers between devices: 26.7 us -> 9.07 us
  starting transfers between devices: 97.1 us -> 114 us
  matrix products: 4.06 us -> 0 us
  local copies, waits for them, and re-layouts: 5.26 us -> 9.16 us
  Pallas kernels: 21.3 us -> 18 us
    ppermute x0 -> x2, starting transfers between devices: none -> 82 us  [the longest x1 74.6 us: body(): lax.ppermute(lax.dynamic_slice_in_dim(plane, (1 - core) * group, group +...]
    ppermute x1, starting transfers between devices: 82 us -> 1.95 us  [body(): lax.ppermute(jnp.concatenate([gate[:1], mult[:1], value[:1]]), COL, down)]
    all_to_all x2, waiting for transfers between devices: 25.9 us -> 0.32 us  [the longest x1 0.32 us: body(): lax.all_to_all(convolved.reshape(chips, CORES * group, width), CHIP, 0, 0...]
    all_to_all x2, starting transfers between devices: 10.4 us -> 26.5 us  [the longest x1 14.9 us: body(): plane = lax.all_to_all(product, CHIP, 0, 0, tiled=True)]
    unnamed x6 -> x42, local copies, waits for them, and re-layouts: 1.29 us -> 9.1 us
    ppermute x1, waiting for transfers between devices: 0.79 us -> 6.77 us  [body(): lax.ppermute(jnp.concatenate([gate[:1], mult[:1], value[:1]]), COL, down)]
    dot_general x1 -> x0, matrix products: 4.06 us -> none  [body(): lax.dot_general(gated, out_weight, (((0,), (0,)), ((), ())), preferred_el...]
    ppermute x0 -> x2, waiting for transfers between devices: none -> 1.97 us  [the longest x1 1.01 us: body(): lax.ppermute(lax.dynamic_slice_in_dim(plane, (1 - core) * group, group +...]
  transfers between devices with their start and end apart: 4 -> 6, of which waited for: 3 -> 4; matrix products, arithmetic and copies ran while one was open for 2% -> 0% of each run, Pallas kernels for 9% -> 7%
where the time goes in v2:
time: 152 us; the launch traced here: 151 us
  starting transfers between devices  114 us (75%)
  Pallas kernels  18 us (12%)
  local copies, waits for them, and re-layouts  9.16 us (6%)
  waiting for transfers between devices  9.07 us (6%)
    ppermute x1, starting transfers between devices, body(): lax.ppermute(lax.dynamic_slice_in_dim(plane, (1 - core) * group, group +...  74.6 us
    all_to_all x1, starting transfers between devices, body(): plane = lax.all_to_all(product, CHIP, 0, 0, tiled=True)  14.9 us
    all_to_all x1, starting transfers between devices, body(): lax.all_to_all(convolved.reshape(chips, CORES * group, width), CHIP, 0, 0...  11.5 us
    pallas_call x1, Pallas kernels, body(): pl.pallas_call(functools.partial(filter_kernel, seq_len=seq_len, width=wi...  10 us
    unnamed x42, local copies, waits for them, and re-layouts  9.1 us
    ppermute x1, starting transfers between devices, body(): other = lax.ppermute(theirs, COL, swap)  7.44 us
    ppermute x1, waiting for transfers between devices, body(): lax.ppermute(jnp.concatenate([gate[:1], mult[:1], value[:1]]), COL, down)  6.77 us
    ppermute x1, starting transfers between devices, body(): lax.ppermute(jnp.concatenate([gate[-1:], mult[-1:], value[-1:]]), COL, up)  3.92 us
  transfers between devices with their start and end apart: 6, of which 4 were waited for; matrix products, arithmetic and copies ran while one was open for 0% of the time, Pallas kernels for 7%

profile of v2, /device:TPU:5, one launch (start us, length us, event | category | flops | bytes accessed | tf_op | source)
XLA Modules:
  0.0 150.9 jit_solution(17969275198589722578)
XLA Ops:
  0.0 2.2 %product.1 = bf16[16,72,128]{2,1,0:T(8,128)(2,1)} custom-call(bf16[128,1024]{1,0:T(8,128)(2,1)} %bitcast.7, bf16[128,1024]{1,0:T(8,128)(2,1)} %bitcast.10, f32[3,1024]{1,0:T(4,128)} %taps_mult.5, f32[3,1024]{1,0:T(4,128)} %taps_value.5), custom_call_target="tpu_custom_call" | custom-call | tf_op jit(solution)/shard_map/product/pallas_call | solution.py:314
  2.2 14.9 %all-to-all-start = ((bf16[16,72,128]{2,1,0:T(8,128)(2,1)}), bf16[16,72,128]{2,1,0:T(8,128)(2,1)S(1)}, u32[]{:S(2)}, u32[]{:S(2)}) async-start(bf16[16,72,128]{2,1,0:T(8,128)(2,1)} %product.1), calls=%async_computation | async-start | bytes 589824 | tf_op jit(solution)/shard_map/all_to_all | solution.py:320
  17.2 0.0 copy-start.6
  17.2 1.0 copy-done.6
  18.2 0.0 copy-start.7
  18.2 1.0 copy-done.7
  19.3 0.0 copy-start.8
  19.3 0.8 copy-done.8
  20.1 0.0 copy-start.9
  20.1 0.7 copy-done.9
  20.9 0.0 copy-start.11
  20.9 0.7 copy-done.11
  21.5 0.0 copy-start.13
  21.5 1.0 copy-done.13
  22.6 0.0 copy-start.16
  22.6 0.8 copy-done.16
  23.3 0.0 copy-start.20
  23.3 0.7 copy-done.20
  24.1 0.0 copy-start.3
  24.1 0.0 copy-start.4
  24.1 0.0 copy-start.14
  24.1 0.0 copy-start.15
  24.1 0.0 copy-start.17
  24.1 0.0 copy-start.18
  24.1 0.0 copy-start.19
  24.1 10.0 %filter.1.spec = f32[1024,256]{1,0:T(8,128)S(1)} custom-call(f32[33,128]{1,0:T(8,128)S(1)} %copy-done.9, f32[128,128]{1,0:T(8,128)S(1)} %copy-done.8, f32[128,1024]{1,0:T(8,128)S(1)} %copy-done.6, f32[128,1024]{1,0:T(8,128)S(1)} %copy-done.7, f32[1,1024]{1,0:T(1,128)S(1)} %bitcast.15, bf16[64,96]{1,0:T(8,128)(2,1)S(1)} %copy-done.20, ...), custom_call_target="tpu_custom_call" | custom-call | flops 4000000000 | bytes 4194304 | tf_op jit(solution)/shard_map/filter/pallas_call | solution.py:324
  34.1 0.0 copy-start.1
  34.1 0.0 copy-start.5
  34.2 0.0 copy-start.2
  34.2 0.0 copy-start.10
  34.2 0.0 copy-start.12
  34.2 0.0 all-to-all-done.plane
  34.2 74.6 %collective-permute-start = (bf16[16,40,128]{2,1,0:T(8,128)(2,1)S(1)}, bf16[16,40,128]{2,1,0:T(8,128)(2,1)S(1)}, u32[]{:S(2)}, u32[]{:S(2)}) collective-permute-start(bf16[16,40,128]{2,1,0:T(8,128)(2,1)S(1)} %constant_dynamic-slice_fusion.1), channel_id=1, source_target_pairs={{0,1},{1,0},{2,3},{3,2},{4,5},{5,4},{6,7},{7,6},{8,9},{9,8},{10,11... | collective-permute-start | bytes 491528 | tf_op jit(solution)/shard_map/ppermute | solution.py:341
  108.8 1.0 collective-permute-done.partner
  109.8 0.0 copy-done.3
  109.8 0.0 copy-done.4
  109.8 0.0 copy-done.14
  109.8 0.0 copy-done.15
  109.8 0.0 copy-done.17
  109.9 0.0 copy-done.18
  109.9 0.0 copy-done.19
  109.9 3.4 %conv.1 = bf16[1024,128]{1,0:T(8,128)(2,1)} custom-call(bf16[16,72,128]{2,1,0:T(8,128)(2,1)S(1)} %all-to-all-done.plane, bf16[16,40,128]{2,1,0:T(8,128)(2,1)S(1)} %collective-permute-done.partner, f32[3,1024]{1,0:T(4,128)S(1)} %copy-done.3, f32[3,1024]{1,0:T(4,128)S(1)} %copy-done.4, f32[1024,256]{1,0:T(8,128)S(1)} %filter.1.spec, ...), custom_call_target="tpu_custom_call" | custom-call | flops 1200000000 | bytes 2097152 | tf_op jit(solution)/shard_map/conv/pallas_call | solution.py:343
  113.2 11.5 %all-to-all-start.1 = ((bf16[16,64,128]{2,1,0:T(8,128)(2,1)}), bf16[16,64,128]{2,1,0:T(8,128)(2,1)S(1)}, u32[]{:S(2)}, u32[]{:S(2)}) async-start(bf16[16,64,128]{2,1,0:T(8,128)(2,1)} %bitcast.4), calls=%async_computation.1 | async-start | bytes 524288 | tf_op jit(solution)/shard_map/all_to_all | solution.py:357
  124.8 0.0 copy-done.1
  124.8 0.0 copy-done.5
  124.8 0.0 copy-done.2
  124.9 3.9 %collective-permute-start.1 = (bf16[3,1024]{1,0:T(4,128)(2,1)S(1)}, bf16[3,1024]{1,0:T(4,128)(2,1)S(1)}, u32[]{:S(2)}, u32[]{:S(2)}) collective-permute-start(bf16[3,1024]{1,0:T(4,128)(2,1)S(1)} %pad_maximum_fusion), channel_id=1, source_target_pairs={{0,1},{1,2},{2,3},{3,4},{4,5},{5,6},{6,7},{7,8},{8,9},{9,10},{10,1... | collective-permute-start | bytes 18440 | tf_op jit(solution)/shard_map/ppermute | solution.py:358
  128.8 2.0 %collective-permute-start.2 = (bf16[3,1024]{1,0:T(4,128)(2,1)S(1)}, bf16[3,1024]{1,0:T(4,128)(2,1)S(1)}, u32[]{:S(2)}, u32[]{:S(2)}) collective-permute-start(bf16[3,1024]{1,0:T(4,128)(2,1)S(1)} %pad_maximum_fusion.1), channel_id=1, source_target_pairs={{1,0},{2,1},{3,2},{4,3},{5,4},{6,5},{7,6},{8,7},{9,8},{10,9},{11,1... | collective-permute-start | bytes 18440 | tf_op jit(solution)/shard_map/ppermute | solution.py:359
  130.8 0.0 collective-permute-done.1.before
  130.8 6.8 %collective-permute-done.2.after = bf16[3,1024]{1,0:T(4,128)(2,1)S(1)} collective-permute-done((bf16[3,1024]{1,0:T(4,128)(2,1)S(1)}, bf16[3,1024]{1,0:T(4,128)(2,1)S(1)}, u32[]{:S(2)}, u32[]{:S(2)}) %collective-permute-start.2) | collective-permute-done | bytes 6176 | tf_op jit(solution)/shard_map/ppermute | solution.py:359
  137.6 0.0 copy-done.10
  137.6 0.0 copy-done.12
  137.6 0.7 gate.1
  138.3 0.3 all-to-all-done.1.planes
  138.6 7.4 %collective-permute-start.3 = (bf16[16,32,128]{2,1,0:T(8,128)(2,1)S(1)}, bf16[16,32,128]{2,1,0:T(8,128)(2,1)S(1)}, u32[]{:S(2)}, u32[]{:S(2)}) collective-permute-start(bf16[16,32,128]{2,1,0:T(8,128)(2,1)S(1)} %constant_dynamic-slice_fusion), channel_id=1, source_target_pairs={{0,1},{1,0},{2,3},{3,2},{4,5},{5,4},{6,7},{7,6},{8,9},{9,8},{10,11... | collective-permute-start | bytes 393224 | tf_op jit(solution)/shard_map/ppermute | solution.py:369
  146.0 1.0 collective-permute-done.3.other
  147.0 0.0 copy-start
  147.0 2.2 %copy-done = bf16[1024,2048]{1,0:T(8,128)(2,1)S(1)} copy-done((bf16[1024,2048]{1,0:T(8,128)(2,1)S(1)}, bf16[1024,2048]{1,0:T(8,128)(2,1)}, u32[]{:S(2)}) %copy-start) | copy-done | bytes 4194328
  149.2 1.7 %mix.1 = bf16[128,2048]{1,0:T(8,128)(2,1)} custom-call(bf16[16,64,128]{2,1,0:T(8,128)(2,1)S(1)} %all-to-all-done.1.planes, bf16[16,32,128]{2,1,0:T(8,128)(2,1)S(1)} %collective-permute-done.3.other, f32[128,1024]{1,0:T(8,128)S(1)} %get-tuple-element.25.gate_part, f32[128,1024]{1,0:T(8,128)S(1)} %get-tuple-element.26.skip_part, bf16[1024,2048]{1,0:T(8,128)(2,1)S(1)} %copy-done), custom_call_target="tpu_custom_call" | custom-call | flops 800000000 | bytes 4194304 | tf_op jit(solution)/shard_map/mix/pallas_call | solution.py:370
  (6 shorter events, 0.1 us)
Async XLA Ops:
  2.2 32.0 %all-to-all-start = ((bf16[16,72,128]{2,1,0:T(8,128)(2,1)}), bf16[16,72,128]{2,1,0:T(8,128)(2,1)S(1)}, u32[]{:S(2)}, u32[]{:S(2)}) async-start(bf16[16,72,128]{2,1,0:T(8,128)(2,1)} %product.1), calls=%async_computation | async-start | bytes 589824 | tf_op jit(solution)/shard_map/all_to_all | solution.py:320
  17.2 1.0 copy-start.6
  18.2 1.0 copy-start.7
  19.3 0.8 copy-start.8
  20.1 0.7 copy-start.9
  20.9 0.7 copy-start.11
  21.5 1.0 copy-start.13
  22.6 0.8 copy-start.16
  23.3 0.7 copy-start.20
  24.1 85.8 %copy-start.3 = (f32[3,1024]{1,0:T(4,128)S(1)}, f32[3,1024]{1,0:T(4,128)}, u32[]{:S(2)}) copy-start(f32[3,1024]{1,0:T(4,128)} %taps_mult.5) | copy-start | bytes 36868
  24.1 85.8 %copy-start.4 = (f32[3,1024]{1,0:T(4,128)S(1)}, f32[3,1024]{1,0:T(4,128)}, u32[]{:S(2)}) copy-start(f32[3,1024]{1,0:T(4,128)} %taps_value.5) | copy-start | bytes 36868
  24.1 85.8 %copy-start.14 = (bf16[2,256,256]{2,1,0:T(8,128)(2,1)S(1)}, bf16[2,256,256]{2,1,0:T(8,128)(2,1)}, u32[]{:S(2)}) copy-start(bf16[2,256,256]{2,1,0:T(8,128)(2,1)} %constant.33.clone.back) | copy-start | bytes 786436
  24.1 85.8 %copy-start.15 = (bf16[2,256,256]{2,1,0:T(8,128)(2,1)S(1)}, bf16[2,256,256]{2,1,0:T(8,128)(2,1)}, u32[]{:S(2)}) copy-start(bf16[2,256,256]{2,1,0:T(8,128)(2,1)} %constant.32.clone.ahead) | copy-start | bytes 786436
  24.1 85.8 %copy-start.17 = (f32[2,32,128]{2,1,0:T(8,128)S(1)}, f32[2,32,128]{2,1,0:T(8,128)}, u32[]{:S(2)}) copy-start(f32[2,32,128]{2,1,0:T(8,128)} %constant.29.clone.refs_6_.twist) | copy-start | bytes 98308
  24.1 85.8 %copy-start.18 = (bf16[32,192]{1,0:T(8,128)(2,1)S(1)}, bf16[32,192]{1,0:T(8,128)(2,1)}, u32[]{:S(2)}) copy-start(bf16[32,192]{1,0:T(8,128)(2,1)} %constant.34.clone.last) | copy-start | bytes 36868
  24.1 85.8 %copy-start.19 = (bf16[64,64]{1,0:T(8,128)(2,1)S(1)}, bf16[64,64]{1,0:T(8,128)(2,1)}, u32[]{:S(2)}) copy-start(bf16[64,64]{1,0:T(8,128)(2,1)} %constant.31.clone.data_first) | copy-start | bytes 24580
  34.1 90.6 %copy-start.1 = (bf16[1,128,1024]{2,1,0:T(8,128)(2,1)S(1)}, bf16[1,128,1024]{2,1,0:T(8,128)(2,1)}, u32[]{:S(2)}) copy-start(bf16[1,128,1024]{2,1,0:T(8,128)(2,1)} %param.21) | copy-start | bytes 786436
  34.1 90.6 %copy-start.5 = (bf16[1,128,1024]{2,1,0:T(8,128)(2,1)S(1)}, bf16[1,128,1024]{2,1,0:T(8,128)(2,1)}, u32[]{:S(2)}) copy-start(bf16[1,128,1024]{2,1,0:T(8,128)(2,1)} %param.20) | copy-start | bytes 786436
  34.2 90.7 %copy-start.2 = (bf16[1,128,1024]{2,1,0:T(8,128)(2,1)S(1)}, bf16[1,128,1024]{2,1,0:T(8,128)(2,1)}, u32[]{:S(2)}) copy-start(bf16[1,128,1024]{2,1,0:T(8,128)(2,1)} %param.22) | copy-start | bytes 786436
  34.2 103.4 %copy-start.10 = (f32[3,1024]{1,0:T(4,128)S(1)}, f32[3,1024]{1,0:T(4,128)}, u32[]{:S(2)}) copy-start(f32[3,1024]{1,0:T(4,128)} %taps_gate.1) | copy-start | bytes 36868
  34.2 103.4 %copy-start.12 = (f32[1024]{0:T(1024)S(1)}, f32[1024]{0:T(1024)}, u32[]{:S(2)}) copy-start(f32[1024]{0:T(1024)} %param.31) | copy-start | bytes 12292
  34.2 75.6 %collective-permute-start = (bf16[16,40,128]{2,1,0:T(8,128)(2,1)S(1)}, bf16[16,40,128]{2,1,0:T(8,128)(2,1)S(1)}, u32[]{:S(2)}, u32[]{:S(2)}) collective-permute-start(bf16[16,40,128]{2,1,0:T(8,128)(2,1)S(1)} %constant_dynamic-slice_fusion.1), channel_id=1, source_target_pairs={{0,1},{1,0},{2,3},{3,2},{4,5},{5,4},{6,7},{7,6},{8,9},{9,8},{10,11... | collective-permute-start | bytes 491528 | tf_op jit(solution)/shard_map/ppermute | solution.py:341
  113.2 25.4 %all-to-all-start.1 = ((bf16[16,64,128]{2,1,0:T(8,128)(2,1)}), bf16[16,64,128]{2,1,0:T(8,128)(2,1)S(1)}, u32[]{:S(2)}, u32[]{:S(2)}) async-start(bf16[16,64,128]{2,1,0:T(8,128)(2,1)} %bitcast.4), calls=%async_computation.1 | async-start | bytes 524288 | tf_op jit(solution)/shard_map/all_to_all | solution.py:357
  124.9 5.9 %collective-permute-start.1 = (bf16[3,1024]{1,0:T(4,128)(2,1)S(1)}, bf16[3,1024]{1,0:T(4,128)(2,1)S(1)}, u32[]{:S(2)}, u32[]{:S(2)}) collective-permute-start(bf16[3,1024]{1,0:T(4,128)(2,1)S(1)} %pad_maximum_fusion), channel_id=1, source_target_pairs={{0,1},{1,2},{2,3},{3,4},{4,5},{5,6},{6,7},{7,8},{8,9},{9,10},{10,1... | collective-permute-start | bytes 18440 | tf_op jit(solution)/shard_map/ppermute | solution.py:358
  128.8 8.7 %collective-permute-start.2 = (bf16[3,1024]{1,0:T(4,128)(2,1)S(1)}, bf16[3,1024]{1,0:T(4,128)(2,1)S(1)}, u32[]{:S(2)}, u32[]{:S(2)}) collective-permute-start(bf16[3,1024]{1,0:T(4,128)(2,1)S(1)} %pad_maximum_fusion.1), channel_id=1, source_target_pairs={{1,0},{2,1},{3,2},{4,3},{5,4},{6,5},{7,6},{8,7},{9,8},{10,9},{11,1... | collective-permute-start | bytes 18440 | tf_op jit(solution)/shard_map/ppermute | solution.py:359
  138.6 8.4 %collective-permute-start.3 = (bf16[16,32,128]{2,1,0:T(8,128)(2,1)S(1)}, bf16[16,32,128]{2,1,0:T(8,128)(2,1)S(1)}, u32[]{:S(2)}, u32[]{:S(2)}) collective-permute-start(bf16[16,32,128]{2,1,0:T(8,128)(2,1)S(1)} %constant_dynamic-slice_fusion), channel_id=1, source_target_pairs={{0,1},{1,0},{2,3},{3,2},{4,5},{5,4},{6,7},{7,6},{8,9},{9,8},{10,11... | collective-permute-start | bytes 393224 | tf_op jit(solution)/shard_map/ppermute | solution.py:369
  147.0 2.2 %copy-start = (bf16[1024,2048]{1,0:T(8,128)(2,1)S(1)}, bf16[1024,2048]{1,0:T(8,128)(2,1)}, u32[]{:S(2)}) copy-start(bf16[1024,2048]{1,0:T(8,128)(2,1)} %weight.1) | copy-start | bytes 12582916

commit v3 on v2

--- a/solution.py
+++ b/solution.py
@@ -15,6 +15,7 @@
 COL = (CHIP, CORE)
 CORES = 2
 EDGE = 8
+ALL_VMEM = 67_000_000
 F32 = jnp.float32
 BF16 = jnp.bfloat16
 
@@ -96,34 +97,40 @@
     return taps[0:1] * up + taps[1:2] * x + taps[2:3] * down
 
 
-def product_kernel(mult, value, taps_mult, taps_value, out):
+def product_kernel(mult, value, gate_head, gate_tail, taps_mult, taps_value, out):
     m, v = mult[...].astype(F32), value[...].astype(F32)
-    zero = jnp.zeros((1, m.shape[1]), F32)
-    product = short(v, zero, zero, taps_value[...]) * short(m, zero, zero, taps_mult[...])
-    product = product.T.astype(BF16)
-    edges = jnp.concatenate([v[:2], m[:2], v[-2:], m[-2:]], axis=0).astype(BF16)
+    product = (short(v, 0.0, 0.0, taps_value[...]) * short(m, 0.0, 0.0, taps_mult[...])).T.astype(BF16)
+    zero = jnp.zeros((EDGE - 6, m.shape[1]), F32)
+    heads = jnp.concatenate([v[:2], m[:2], gate_head[...].astype(F32)[:2], zero], axis=0)
+    tails = jnp.concatenate([v[-2:], m[-2:], gate_tail[...].astype(F32)[-2:], zero], axis=0)
     chips, rows, width = out.shape
-    part = (rows - EDGE) // 2
+    part = (rows - EDGE) // CORES
+    half = CORES * part
+    low = lax.broadcasted_iota(jnp.int32, (EDGE, width), 1) < half
     for k in range(chips):
-        at = 2 * part * k
+        at = half * k
         lane = at // width * width
+        head, tail = heads[:, lane : lane + width], tails[:, lane : lane + width]
+        if at == lane:
+            tail = pltpu.roll(tail, half, 1)
+        else:
+            head = pltpu.roll(head, half, 1)
         out[k, :part, :] = product[at : at + part]
-        out[k, part : part + EDGE, :] = edges[:, lane : lane + width]
-        out[k, part + EDGE :, :] = product[at + part : at + 2 * part]
-
-
-def gate_kernel(
-    gate, mult, value, before, after, taps_gate, taps_mult, taps_value, skip, gate_out, skip_out
-):
-    b, a = before[...].astype(F32), after[...].astype(F32)
-    g = short(gate[...].astype(F32), b[0:1], a[0:1], taps_gate[...])
-    m = short(mult[...].astype(F32), b[1:2], a[1:2], taps_mult[...])
-    v = short(value[...].astype(F32), b[2:3], a[2:3], taps_value[...])
-    gate_out[...] = g
-    skip_out[...] = skip[...] * (v * m)
-
-
-def mix_kernel(planes, other, gate_part, skip_part, weight, out, stage):
+        out[k, part : part + EDGE, :] = jnp.where(low, head, tail).astype(BF16)
+        out[k, part + EDGE :, :] = product[at + part : at + half]
+
+
+def gains_kernel(taps_mult, taps_value, taps_gate, skip, out):
+    width = out.shape[1]
+    group = width // 4
+    channel = (lax.axis_index(CHIP) * CORES + lax.axis_index(CORE)) * group
+    lane = pl.multiple_of(channel // width * width, width)
+    gains = [r[:, pl.ds(lane, width)] for r in (taps_mult, taps_value, taps_gate, skip)]
+    gains = jnp.concatenate(gains + [jnp.zeros((out.shape[0] - 10, width), F32)], axis=0)
+    out[...] = pltpu.roll(gains, (width - channel % width) % width, 1)
+
+
+def mix_kernel(planes, other, gate, mult, value, taps_gate, taps_mult, taps_value, skip, weight, out, stage):
     core = lax.axis_index(CORE)
     chips, rows, _ = planes.shape
     group = rows // CORES
@@ -132,7 +139,12 @@
         far = pl.multiple_of(rows * k + (1 - core) * group, group)
         stage[pl.ds(near, group), :] = planes[k, pl.ds(pl.multiple_of(core * group, group), group), :].astype(F32)
         stage[pl.ds(far, group), :] = other[k].astype(F32)
-    gated = ((stage[...].T + skip_part[...]) * gate_part[...]).astype(BF16)
+    q = stage[...].T
+    row = lax.broadcasted_iota(jnp.int32, q.shape, 0)
+    border = (row == 0) | (row == q.shape[0] - 1)
+    product = short(value[...].astype(F32), 0.0, 0.0, taps_value[...]) * short(mult[...].astype(F32), 0.0, 0.0, taps_mult[...])
+    g = short(gate[...].astype(F32), 0.0, 0.0, taps_gate[...])
+    gated = jnp.where(border, q, (q + skip[...] * product) * g).astype(BF16)
     out[...] = dot(gated, weight[...]).astype(BF16)
 
 
@@ -222,12 +234,12 @@
 
 
 def conv_kernel(
-    plane, partner, taps_mult, taps_value, spec, data_first, twist, ahead, back, last, out, stage, left_high, left_low,
-    *, group
+    plane, partner, gains, spec, data_first, twist, ahead, back, last,
+    out, stage, left_high, left_low, *, group
 ):
     chips, rows, width = partner.shape
     blocks = chips * CORES
-    chip, core = lax.axis_index(CHIP), lax.axis_index(CORE)
+    core = lax.axis_index(CORE)
     pitch = group + 2 * EDGE
     base = pl.multiple_of(EDGE * (1 - core), EDGE)
     own_at = pl.multiple_of(core * group, group)
@@ -237,11 +249,13 @@
         stage[pl.ds(near, rows), :] = plane[k, pl.ds(own_at, rows), :].astype(F32)
         stage[pl.ds(far, rows), :] = partner[k].astype(F32)
 
-    channel = (chip * CORES + core) * group
-    lane = pl.multiple_of(channel // width * width, width)
-    tm, tv = taps_mult[:, pl.ds(lane, width)], taps_value[:, pl.ds(lane, width)]
+    tm, tv, tg, gain = gains[0:3], gains[3:6], gains[6:9], gains[9:10]
     edge_at = (group + EDGE) * (1 - core)
-    v0, v1, m0, m1, v2, v3, m2, m3 = [stage[pl.ds(edge_at + q, blocks, stride=pitch), :] for q in range(EDGE)]
+    first = [
+        pltpu.roll(stage[pl.ds(edge_at + q, blocks, stride=pitch), :], (width - core * group) % width, 1) for q in range(6)
+    ]
+    v0, v1, m0, m1, g0, g1 = first
+    v2, v3, m2, m3, g2, g3 = [pltpu.roll(x, width - CORES * group, 1) for x in first]
     row = lax.broadcasted_iota(jnp.int32, (blocks, width), 0)
     column = lax.broadcasted_iota(jnp.int32, (blocks, width), 1)
 
@@ -252,19 +266,26 @@
         after = jnp.where(row == blocks - 1, 0.0, pltpu.roll(following, blocks - 1, 0))
         return t[0:1] * previous + t[1:2] * x + t[2:3] * after
 
+    odd = column % 2 == 1
+
+    def pair(heads, tails):
+        tails = pltpu.roll(tails, width - 1, 1)
+        return jnp.where(odd, tails, heads), jnp.where(odd, heads, tails)
+
+    def at_ends(pairs, c):
+        return pltpu.roll(pairs[c % 2], (width - c) % width, 1)
+
     heads = head(tv, v3, v0, v1) * head(tm, m3, m0, m1)
     tails = tail(tv, v2, v3, v0) * tail(tm, m2, m3, m0)
-    shift = width - channel % width
-    heads = pltpu.roll(heads, shift, 1)
-    tails = pltpu.roll(tails, shift + width - 1, 1)
-    odd = column % 2 == 1
-    edges = (jnp.where(odd, tails, heads), jnp.where(odd, heads, tails))
+    edges = pair(heads, tails)
+    skips = pair(gain * heads, gain * tails)
+    gates = pair(head(tg, g3, g0, g1), tail(tg, g2, g3, g0))
     border = (column == 0) | (column == width - 1)
 
     cos, sin = twist[0], twist[1]
     for c in range(group):
         x = stage[pl.ds(EDGE + c, blocks, stride=pitch), :]
-        x = jnp.where(border, pltpu.roll(edges[c % 2], (width - c) % width, 1), x).astype(BF16)
+        x = jnp.where(border, at_ends(edges, c), x).astype(BF16)
         z = dot(data_first[...], jnp.concatenate([x, x], axis=0))
         re, im = z[:blocks], z[blocks:]
         left = jnp.concatenate([re * cos + im * sin, im * cos - re * sin], axis=1)
@@ -280,7 +301,9 @@
         vr = v[c * blocks : (c + 1) * blocks, :width]
         vi = v[c * blocks : (c + 1) * blocks, width:]
         high, low = halves(jnp.concatenate([vr * cos - vi * sin, vi * cos + vr * sin], axis=0))
-        stage[pl.ds(c, blocks, stride=group), :] = dot(last[...], jnp.concatenate([high, low, high], axis=0))
+        y = dot(last[...], jnp.concatenate([high, low, high], axis=0))
+        y = jnp.where(border, (y + at_ends(skips, c)) * at_ends(gates, c), y)
+        stage[pl.ds(c, blocks, stride=group), :] = y
     out[...] = stage[: blocks * group, :].astype(BF16)
 
 
@@ -307,16 +330,27 @@
     gate, mult, value = gate_in[0], mult_in[0], value_in[0]
     t = tables(cols, width)
     swap = [(i, i + 1 - 2 * (i % CORES)) for i in range(cols)]
-    up = [(i, i + 1) for i in range(cols - 1)]
-    down = [(j, i) for i, j in up]
 
     rows = CORES * group + EDGE
+    theirs_at = ((1 - core) * group).astype(jnp.uint32)
+    whole = lambda x: pl.BlockSpec(x.shape, lambda i: (0, 0))
+    strip = 16
     product = pl.pallas_call(
         product_kernel,
+        grid=(1,),
+        in_specs=[
+            whole(mult),
+            whole(value),
+            pl.BlockSpec((strip, channels), lambda i: (0, 0)),
+            pl.BlockSpec((strip, channels), lambda i: (width // strip - 1, 0)),
+            whole(taps_mult),
+            whole(taps_value),
+        ],
+        out_specs=pl.BlockSpec((chips, rows, width), lambda i: (0, 0, 0)),
         out_shape=jax.ShapeDtypeStruct((chips, rows, width), BF16),
-        compiler_params=pltpu.CompilerParams(vmem_limit_bytes=67_000_000),
+        compiler_params=pltpu.CompilerParams(vmem_limit_bytes=ALL_VMEM),
         name="product",
-    )(mult, value, taps_mult, taps_value)
+    )(mult, value, gate, gate, taps_mult, taps_value)
     plane = lax.all_to_all(product, CHIP, 0, 0, tiled=True)
     filter_args = (
         filter_first, filter_second, filter_ahead, filter_behind, filter_decay[None], t["kernel_first"], t["twist"], t["both"]
@@ -333,12 +367,20 @@
             pltpu.VMEM((group * cols, 4 * width), BF16),
             pltpu.SemaphoreType.DMA((len(filter_args),)),
         ],
-        compiler_params=limit(16),
+        compiler_params=pltpu.CompilerParams(vmem_limit_bytes=ALL_VMEM),
         cost_estimate=cost(10, 2**22),
         name="filter",
     )(*filter_args)
-    plane, spec = lax.optimization_barrier((plane, spec))
-    partner = lax.ppermute(lax.dynamic_slice_in_dim(plane, (1 - core) * group, group + EDGE, 1), COL, swap)
+    spec, taps_near, gain_near = lax.optimization_barrier((spec, (taps_mult, taps_value, taps_gate), skip_gain[None]))
+    gains = pl.pallas_call(
+        gains_kernel,
+        out_shape=jax.ShapeDtypeStruct((16, width), F32),
+        compiler_params=limit(1),
+        cost_estimate=cost(20, 2**21),
+        name="gains",
+    )(*taps_near, gain_near)
+    plane, spec, gains = lax.optimization_barrier((plane, spec, gains))
+    partner = lax.ppermute(lax.dynamic_slice_in_dim(plane, theirs_at, group + EDGE, 1), COL, swap)
 
     convolved = pl.pallas_call(
         functools.partial(conv_kernel, group=group),
@@ -351,21 +393,10 @@
         compiler_params=limit(16),
         cost_estimate=cost(3, 2**21),
         name="conv",
-    )(plane, partner, taps_mult, taps_value, spec, t["data_first"], t["twist"], t["ahead"], t["back"], t["last"])
-
-    convolved, gate, mult, value = lax.optimization_barrier((convolved, gate, mult, value))
+    )(plane, partner, gains, spec, t["data_first"], t["twist"], t["ahead"], t["back"], t["last"])
+
     planes = lax.all_to_all(convolved.reshape(chips, CORES * group, width), CHIP, 0, 0, tiled=True)
-    before = lax.ppermute(jnp.concatenate([gate[-1:], mult[-1:], value[-1:]]), COL, up)
-    after = lax.ppermute(jnp.concatenate([gate[:1], mult[:1], value[:1]]), COL, down)
-    gate_part, skip_part = pl.pallas_call(
-        gate_kernel,
-        out_shape=[jax.ShapeDtypeStruct((width, channels), F32)] * 2,
-        compiler_params=limit(12),
-        cost_estimate=cost(20, 2**21),
-        name="gate",
-    )(gate, mult, value, before, after, taps_gate, taps_mult, taps_value, skip_gain[None])
-    planes, gate_part, skip_part = lax.optimization_barrier((planes, gate_part, skip_part))
-    theirs = lax.dynamic_slice_in_dim(planes, (1 - core) * group, group, 1)
+    theirs = lax.dynamic_slice_in_dim(planes, theirs_at, group, 1)
     other = lax.ppermute(theirs, COL, swap)
     mixed = pl.pallas_call(
         mix_kernel,
@@ -374,7 +405,7 @@
         compiler_params=limit(12),
         cost_estimate=cost(2, 2**22),
         name="mix",
-    )(planes, other, gate_part, skip_part, out_weight)
+    )(planes, other, gate, mult, value, taps_gate, taps_mult, taps_value, skip_gain[None], out_weight)
     return mixed[None]
 
 

time: 152 us -> 147 us (0.967)
  blocking collectives: 0 us -> 24.5 us
  starting transfers between devices: 114 us -> 97.8 us
  local copies, waits for them, and re-layouts: 9.16 us -> 1.96 us
  waiting for transfers between devices: 9.07 us -> 1.97 us
  Pallas kernels: 18 us -> 20.5 us
    all_to_all x0 -> x1, blocking collectives: none -> 24.5 us  [body(): lax.all_to_all(convolved.reshape(chips, CORES * group, width), CHIP, 0, 0...]
    all_to_all x1 -> x0, starting transfers between devices: 11.5 us -> none  [body(): lax.all_to_all(convolved.reshape(chips, CORES * group, width), CHIP, 0, 0...]
    unnamed x42 -> x30, local copies, waits for them, and re-layouts: 9.1 us -> 0.78 us
    ppermute x3 -> x1, waiting for transfers between devices: 7.78 us -> 1.01 us  [body(): lax.ppermute(lax.dynamic_slice_in_dim(plane, theirs_at, group + EDGE, 1),...]
    ppermute x3 -> x1, starting transfers between devices: 80.4 us -> 75.8 us  [body(): lax.ppermute(lax.dynamic_slice_in_dim(plane, theirs_at, group + EDGE, 1),...]
    pallas_call x1, Pallas kernels: 10 us -> 12.2 us  [body(): pl.pallas_call(functools.partial(filter_kernel, seq_len=seq_len, width=wi...]
  transfers between devices with their start and end apart: 6 -> 3, of which waited for: 4 -> 2; matrix products, arithmetic and copies ran while one was open for 0% -> 0% of each run, Pallas kernels for 7% -> 8%
where the time goes in v3:
time: 147 us
  starting transfers between devices  97.8 us (67%)
  blocking collectives  24.5 us (17%)
  Pallas kernels  20.5 us (14%)
  waiting for transfers between devices  1.97 us (1%)
  local copies, waits for them, and re-layouts  1.96 us (1%)
    ppermute x1, starting transfers between devices, body(): lax.ppermute(lax.dynamic_slice_in_dim(plane, theirs_at, group + EDGE, 1),...  75.8 us
    all_to_all x1, blocking collectives, body(): lax.all_to_all(convolved.reshape(chips, CORES * group, width), CHIP, 0, 0...  24.5 us
    all_to_all x1, starting transfers between devices, body(): plane = lax.all_to_all(product, CHIP, 0, 0, tiled=True)  14.9 us
    pallas_call x1, Pallas kernels, body(): pl.pallas_call(functools.partial(filter_kernel, seq_len=seq_len, width=wi...  12.2 us
    ppermute x1, starting transfers between devices, body(): other = lax.ppermute(theirs, COL, swap)  7.08 us
    pallas_call x1, Pallas kernels, body(): pl.pallas_call(functools.partial(conv_kernel, group=group), out_shape=jax...  3.81 us
  transfers between devices with their start and end apart: 3, of which 2 were waited for; matrix products, arithmetic and copies ran while one was open for 0% of the time, Pallas kernels for 8%

profile of v3, /device:TPU:5, one launch (start us, length us, event | category | flops | bytes accessed | tf_op | source)
XLA Modules:
  0.0 147.0 jit_solution(18020153574804075387)
XLA Ops:
  0.0 2.3 %product.1 = bf16[16,72,128]{2,1,0:T(8,128)(2,1)} custom-call(bf16[128,1024]{1,0:T(8,128)(2,1)} %bitcast.10, bf16[128,1024]{1,0:T(8,128)(2,1)} %bitcast.12, bf16[128,1024]{1,0:T(8,128)(2,1)} %bitcast.7, bf16[128,1024]{1,0:T(8,128)(2,1)} %bitcast.8, f32[3,1024]{1,0:T(4,128)} %taps_mult.4, f32[3,1024]{1,0:T(4,128)} %taps_value.4), custom_call_target="tpu_custom_call" | custom-call | tf_op jit(solution)/shard_map/product/pallas_call | solution.py:338
  2.3 14.9 %all-to-all-start = ((bf16[16,72,128]{2,1,0:T(8,128)(2,1)}), bf16[16,72,128]{2,1,0:T(8,128)(2,1)}, u32[]{:S(2)}, u32[]{:S(2)}) async-start(bf16[16,72,128]{2,1,0:T(8,128)(2,1)} %product.1), calls=%async_computation | async-start | bytes 589824 | tf_op jit(solution)/shard_map/all_to_all | solution.py:354
  17.3 0.0 copy-start.4
  17.3 0.0 copy-start.5
  17.3 0.0 copy-start.8
  17.3 12.2 %filter.1.spec = f32[1024,256]{1,0:T(8,128)} custom-call(f32[33,128]{1,0:T(8,128)} %refs_0_.1, f32[128,128]{1,0:T(8,128)} %refs_1_.1, f32[128,1024]{1,0:T(8,128)} %refs_2_.1, f32[128,1024]{1,0:T(8,128)} %refs_3_.1, f32[1,1024]{1,0:T(1,128)} %bitcast.17, bf16[64,96]{1,0:T(8,128)(2,1)} %constant.24.clone.refs_5_, f32[2,32,128]{2,1,0:T(8,128)} %constant.25.clone.refs_6_.twist, ...), custom_call_target="tpu_custom_call" | custom-call | flops 4000000000 | bytes 4194304 | tf_op jit(solution)/shard_map/filter/pallas_call | solution.py:358
  29.5 0.0 copy-done.4
  29.5 0.0 copy-done.5
  29.5 0.0 copy-done.8
  29.5 0.0 copy-start.6
  29.5 0.7 copy-done.6
  30.2 0.0 copy-start.9
  30.2 0.0 copy-start.10
  30.2 0.0 copy-start.11
  30.2 0.0 copy-start.12
  30.2 0.0 copy-start.13
  30.2 0.0 copy-start.14
  30.2 0.1 gains.1
  30.3 0.0 copy-start.1
  30.3 0.0 copy-start.2
  30.3 0.0 copy-start.3
  30.3 0.0 copy-start.7
  30.4 0.0 all-to-all-done.plane
  30.4 0.0 copy-start
  30.4 1.1 constant_dynamic-slice_fusion.1
  31.5 75.8 %collective-permute-start = (bf16[16,40,128]{2,1,0:T(8,128)(2,1)S(1)}, bf16[16,40,128]{2,1,0:T(8,128)(2,1)S(1)}, u32[]{:S(2)}, u32[]{:S(2)}) collective-permute-start(bf16[16,40,128]{2,1,0:T(8,128)(2,1)S(1)} %constant_dynamic-slice_fusion.1), channel_id=1, source_target_pairs={{0,1},{1,0},{2,3},{3,2},{4,5},{5,4},{6,7},{7,6},{8,9},{9,8},{10,11... | collective-permute-start | bytes 491528 | tf_op jit(solution)/shard_map/ppermute | solution.py:383
  107.4 1.0 collective-permute-done.partner
  108.4 0.0 copy-done.9
  108.4 0.0 copy-done.10
  108.4 0.0 copy-done.11
  108.4 0.0 copy-done.12
  108.4 0.0 copy-done.13
  108.4 0.0 copy-done.14
  108.4 3.8 %conv.1 = bf16[1024,128]{1,0:T(8,128)(2,1)S(1)} custom-call(bf16[16,72,128]{2,1,0:T(8,128)(2,1)} %all-to-all-done.plane, bf16[16,40,128]{2,1,0:T(8,128)(2,1)S(1)} %collective-permute-done.partner, f32[16,128]{1,0:T(8,128)S(1)} %gains.1, f32[1024,256]{1,0:T(8,128)S(1)} %copy-done.14, bf16[64,64]{1,0:T(8,128)(2,1)S(1)} %copy-done.13, ...), custom_call_target="tpu_custom_call" | custom-call | flops 1200000000 | bytes 2097152 | tf_op jit(solution)/shard_map/conv/pallas_call | solution.py:385
  112.2 24.5 %all_to_all.10.planes = bf16[16,64,128]{2,1,0:T(8,128)(2,1)S(1)} all-to-all(bf16[16,64,128]{2,1,0:T(8,128)(2,1)S(1)} %bitcast.14), channel_id=1, replica_groups=mesh['grp'=2,'row'=16,'col_chip'=16,'col_core'=2] {'col_chip'}, dimensions={0} | all-to-all | bytes 524288 | tf_op jit(solution)/shard_map/all_to_all | solution.py:398
  136.7 7.1 %collective-permute-start.1 = (bf16[16,32,128]{2,1,0:T(8,128)(2,1)S(1)}, bf16[16,32,128]{2,1,0:T(8,128)(2,1)S(1)}, u32[]{:S(2)}, u32[]{:S(2)}) collective-permute-start(bf16[16,32,128]{2,1,0:T(8,128)(2,1)S(1)} %constant_dynamic-slice_fusion), channel_id=1, source_target_pairs={{0,1},{1,0},{2,3},{3,2},{4,5},{5,4},{6,7},{7,6},{8,9},{9,8},{10,11... | collective-permute-start | bytes 393224 | tf_op jit(solution)/shard_map/ppermute | solution.py:400
  143.8 1.0 collective-permute-done.1.other
  144.8 0.0 copy-done.1
  144.8 0.0 copy-done.2
  144.8 0.0 copy-done.3
  144.8 0.0 copy-done.7
  144.8 0.0 copy-done
  144.8 2.2 %mix.1 = bf16[128,2048]{1,0:T(8,128)(2,1)} custom-call(bf16[16,64,128]{2,1,0:T(8,128)(2,1)S(1)} %all_to_all.10.planes, bf16[16,32,128]{2,1,0:T(8,128)(2,1)S(1)} %collective-permute-done.1.other, bf16[128,1024]{1,0:T(8,128)(2,1)S(1)} %bitcast.9, bf16[128,1024]{1,0:T(8,128)(2,1)S(1)} %bitcast.11, bf16[128,1024]{1,0:T(8,128)(2,1)S(1)} %bitcast.13, ...), custom_call_target="tpu_custom_call" | custom-call | flops 800000000 | bytes 4194304 | tf_op jit(solution)/shard_map/mix/pallas_call | solution.py:401
  (1 shorter events, 0.0 us)
Async XLA Ops:
  2.3 28.1 %all-to-all-start = ((bf16[16,72,128]{2,1,0:T(8,128)(2,1)}), bf16[16,72,128]{2,1,0:T(8,128)(2,1)}, u32[]{:S(2)}, u32[]{:S(2)}) async-start(bf16[16,72,128]{2,1,0:T(8,128)(2,1)} %product.1), calls=%async_computation | async-start | bytes 589824 | tf_op jit(solution)/shard_map/all_to_all | solution.py:354
  17.3 12.2 %copy-start.4 = (f32[3,1024]{1,0:T(4,128)S(1)}, f32[3,1024]{1,0:T(4,128)}, u32[]{:S(2)}) copy-start(f32[3,1024]{1,0:T(4,128)} %taps_mult.4) | copy-start | bytes 36868
  17.3 12.2 %copy-start.5 = (f32[3,1024]{1,0:T(4,128)S(1)}, f32[3,1024]{1,0:T(4,128)}, u32[]{:S(2)}) copy-start(f32[3,1024]{1,0:T(4,128)} %taps_value.4) | copy-start | bytes 36868
  17.3 12.2 %copy-start.8 = (f32[1024]{0:T(1024)S(1)}, f32[1024]{0:T(1024)}, u32[]{:S(2)}) copy-start(f32[1024]{0:T(1024)} %param.31) | copy-start | bytes 12292
  29.5 0.7 copy-start.6
  30.2 78.1 %copy-start.9 = (bf16[2,256,256]{2,1,0:T(8,128)(2,1)S(1)}, bf16[2,256,256]{2,1,0:T(8,128)(2,1)}, u32[]{:S(2)}) copy-start(bf16[2,256,256]{2,1,0:T(8,128)(2,1)} %constant.29.clone.back) | copy-start | bytes 786436
  30.2 78.2 %copy-start.10 = (bf16[2,256,256]{2,1,0:T(8,128)(2,1)S(1)}, bf16[2,256,256]{2,1,0:T(8,128)(2,1)}, u32[]{:S(2)}) copy-start(bf16[2,256,256]{2,1,0:T(8,128)(2,1)} %constant.28.clone.ahead) | copy-start | bytes 786436
  30.2 78.2 %copy-start.11 = (f32[2,32,128]{2,1,0:T(8,128)S(1)}, f32[2,32,128]{2,1,0:T(8,128)}, u32[]{:S(2)}) copy-start(f32[2,32,128]{2,1,0:T(8,128)} %constant.25.clone.refs_6_.twist) | copy-start | bytes 98308
  30.2 78.2 %copy-start.12 = (bf16[32,192]{1,0:T(8,128)(2,1)S(1)}, bf16[32,192]{1,0:T(8,128)(2,1)}, u32[]{:S(2)}) copy-start(bf16[32,192]{1,0:T(8,128)(2,1)} %constant.30.clone.last) | copy-start | bytes 36868
  30.2 78.2 %copy-start.13 = (bf16[64,64]{1,0:T(8,128)(2,1)S(1)}, bf16[64,64]{1,0:T(8,128)(2,1)}, u32[]{:S(2)}) copy-start(bf16[64,64]{1,0:T(8,128)(2,1)} %constant.27.clone.data_first) | copy-start | bytes 24580
  30.2 78.1 %copy-start.14 = (f32[1024,256]{1,0:T(8,128)S(1)}, f32[1024,256]{1,0:T(8,128)}, u32[]{:S(2)}) copy-start(f32[1024,256]{1,0:T(8,128)} %filter.1.spec) | copy-start | bytes 3145732
  30.3 114.4 %copy-start.1 = (bf16[1,128,1024]{2,1,0:T(8,128)(2,1)S(1)}, bf16[1,128,1024]{2,1,0:T(8,128)(2,1)}, u32[]{:S(2)}) copy-start(bf16[1,128,1024]{2,1,0:T(8,128)(2,1)} %param.20) | copy-start | bytes 786436
  30.3 114.4 %copy-start.2 = (bf16[1,128,1024]{2,1,0:T(8,128)(2,1)S(1)}, bf16[1,128,1024]{2,1,0:T(8,128)(2,1)}, u32[]{:S(2)}) copy-start(bf16[1,128,1024]{2,1,0:T(8,128)(2,1)} %param.21) | copy-start | bytes 786436
  30.3 114.4 %copy-start.3 = (bf16[1,128,1024]{2,1,0:T(8,128)(2,1)S(1)}, bf16[1,128,1024]{2,1,0:T(8,128)(2,1)}, u32[]{:S(2)}) copy-start(bf16[1,128,1024]{2,1,0:T(8,128)(2,1)} %param.22) | copy-start | bytes 786436
  30.3 114.5 %copy-start.7 = (f32[3,1024]{1,0:T(4,128)S(1)}, f32[3,1024]{1,0:T(4,128)}, u32[]{:S(2)}) copy-start(f32[3,1024]{1,0:T(4,128)} %taps_gate.2) | copy-start | bytes 36868
  30.4 114.4 %copy-start = (bf16[1024,2048]{1,0:T(8,128)(2,1)S(1)}, bf16[1024,2048]{1,0:T(8,128)(2,1)}, u32[]{:S(2)}) copy-start(bf16[1024,2048]{1,0:T(8,128)(2,1)} %weight.1) | copy-start | bytes 12582916
  31.5 76.8 %collective-permute-start = (bf16[16,40,128]{2,1,0:T(8,128)(2,1)S(1)}, bf16[16,40,128]{2,1,0:T(8,128)(2,1)S(1)}, u32[]{:S(2)}, u32[]{:S(2)}) collective-permute-start(bf16[16,40,128]{2,1,0:T(8,128)(2,1)S(1)} %constant_dynamic-slice_fusion.1), channel_id=1, source_target_pairs={{0,1},{1,0},{2,3},{3,2},{4,5},{5,4},{6,7},{7,6},{8,9},{9,8},{10,11... | collective-permute-start | bytes 491528 | tf_op jit(solution)/shard_map/ppermute | solution.py:383
  136.7 8.0 %collective-permute-start.1 = (bf16[16,32,128]{2,1,0:T(8,128)(2,1)S(1)}, bf16[16,32,128]{2,1,0:T(8,128)(2,1)S(1)}, u32[]{:S(2)}, u32[]{:S(2)}) collective-permute-start(bf16[16,32,128]{2,1,0:T(8,128)(2,1)S(1)} %constant_dynamic-slice_fusion), channel_id=1, source_target_pairs={{0,1},{1,0},{2,3},{3,2},{4,5},{5,4},{6,7},{7,6},{8,9},{9,8},{10,11... | collective-permute-start | bytes 393224 | tf_op jit(solution)/shard_map/ppermute | solution.py:400

commit v4 on v3

--- a/solution.py
+++ b/solution.py
@@ -19,27 +19,27 @@
 F32 = jnp.float32
 BF16 = jnp.bfloat16
 
-TWO_PI_HEAD = np.float32(np.round(2.0 * math.pi * 2**14) / 2**14)
-TWO_PI_TAIL = np.float32(2.0 * math.pi - float(TWO_PI_HEAD))
-
-
-def sine_coefficients():
-    nodes = np.cos((np.arange(4000) + 0.5) * math.pi / 8000) * math.pi * 1.0001
-    basis = np.stack([nodes ** (2 * j + 1) for j in range(7)], axis=1)
-    return [float(v) for v in np.linalg.lstsq(basis, np.sin(nodes), rcond=None)[0]]
-
-
-SINE = sine_coefficients()
-
-
-def sine(x):
-    turns = jnp.floor(x * np.float32(0.5 / math.pi) + 0.5)
-    r = (x - turns * TWO_PI_HEAD) - turns * TWO_PI_TAIL
-    z = r * r
-    total = np.float32(SINE[6]) * z + np.float32(SINE[5])
-    for j in (4, 3, 2, 1, 0):
-        total = total * z + np.float32(SINE[j])
-    return total * r
+def sine_coefficients(terms):
+    nodes = np.cos((np.arange(4000) + 0.5) * math.pi / 8000) * 0.25
+    basis = np.stack([nodes ** (2 * j + 1) for j in range(terms)], axis=1)
+    return [np.float32(v) for v in np.linalg.lstsq(basis, np.sin(2.0 * math.pi * nodes), rcond=None)[0]]
+
+
+SINE = sine_coefficients(4)
+QUARTER = np.float32(0.25)
+
+
+def cosine_of_turns(u):
+    w = QUARTER - jnp.abs(u - jnp.round(u))
+    z = w * w
+    total = SINE[-1] * z + SINE[-2]
+    for c in SINE[-3::-1]:
+        total = total * z + c
+    return total * w
+
+
+def sine_of_turns(t):
+    return cosine_of_turns(t - QUARTER)
 
 
 def halves(x):
@@ -151,21 +151,22 @@
 def filter_kernel(
     *refs, seq_len, width, chunk, group
 ):
-    sources, out, copies, (own, stage, left_high, left_low, sems) = refs[:8], refs[8], refs[9:17], refs[17:]
+    sources, out, copies, (own, stage, left_high, left_low, result, sems, out_sems) = refs[:8], refs[8], refs[9:17], refs[17:]
+    channel = (lax.axis_index(CHIP) * CORES + lax.axis_index(CORE)) * group
+    lane = pl.multiple_of(channel // width * width, width)
+    row_at = pl.multiple_of(channel % width, group)
+    sources = [x.at[:, pl.ds(lane, width)] if n in (2, 3, 4) else x for n, x in enumerate(sources)]
     moves = [pltpu.make_async_copy(a, b, sems.at[n]) for n, (a, b) in enumerate(zip(sources, copies))]
     for move in moves:
         move.start()
-    for move in moves:
+    for move in moves[:5]:
         move.wait()
     first, second, ahead, behind, decay, kernel_first, twist, both = copies
     hidden = second.shape[0]
     bands = (first.shape[0] - 1) // 2
-    channel = (lax.axis_index(CHIP) * CORES + lax.axis_index(CORE)) * group
-    lane = pl.multiple_of(channel // width * width, width)
-    row_at = pl.multiple_of(channel % width, group)
-    own[0] = ahead[:, pl.ds(lane, width)].T
-    own[1] = behind[:, pl.ds(lane, width)].T
-    own[2] = jnp.broadcast_to(decay[:, pl.ds(lane, width)], (width, width)).T
+    own[0] = ahead[...].T
+    own[1] = behind[...].T
+    own[2] = jnp.broadcast_to(decay[...], (width, width)).T
     sides = jnp.concatenate([own[0, pl.ds(row_at, group), :], own[1, pl.ds(row_at, group), :]], axis=0)
     rates = own[2, pl.ds(row_at, group), :][:, 0:1]
     rates = jnp.concatenate([rates, rates], axis=0)
@@ -174,11 +175,11 @@
     w1 = jnp.concatenate(
         [first[1 : 1 + 2 * bands, :], first[0:1, :], jnp.zeros((padded - 2 * bands - 1, hidden), F32)], axis=0
     )
-    w1h, w1l = halves(w1)
+    w1h, w1l = halves(w1 * np.float32(0.5 / math.pi))
     w1s = jnp.concatenate(
         [w1h.astype(F32), w1h.astype(F32), w1l.astype(F32), jnp.zeros((128 - 3 * padded, hidden), F32)], axis=0
     ).T.astype(BF16)
-    w2h, w2l = halves(second[...].T)
+    w2h, w2l = halves(second[...].T * np.float32(0.5 / math.pi))
     w2s = jnp.concatenate([w2h, w2h, w2l], axis=1)
     w3h, w3l = halves(sides)
     w3s = jnp.concatenate([w3h, w3h, w3l], axis=1)
@@ -186,22 +187,21 @@
     band_at = jnp.where(row < bands, row, row - bands).astype(F32)
     band = np.float32(0.0001) + band_at * np.float32((bands - 1 - 0.0001) / (bands - 1))
     band = jnp.where(row < bands, band, -band)
-    offset = jnp.where(row < bands, np.float32(0.5 * math.pi), np.float32(0.0))
+    offset = jnp.where(row < bands, np.float32(0.0), -QUARTER)
     head_row = lax.broadcasted_iota(jnp.int32, (8, chunk), 0)
 
     def step(i, total):
         at = i * chunk
         position = (lax.broadcasted_iota(jnp.int32, (1, chunk), 1) + at).astype(F32)
         tau = position / np.float32(seq_len - 1)
-        omega = position * np.float32(2.0 * math.pi / seq_len)
-        trig = sine(omega * band + offset)
+        trig = cosine_of_turns(position * np.float32(1.0 / seq_len) * band + offset)
         feats = jnp.concatenate([trig, jnp.where(head_row == 0, tau, 0.0)], axis=0)
         fh = feats.astype(BF16).astype(F32)
         fs = jnp.concatenate(
             [fh, feats - fh, fh, jnp.zeros((128 - 3 * padded, chunk), F32)], axis=0
         ).astype(BF16)
-        h1h, h1l = halves(sine(dot(w1s, fs)))
-        h2h, h2l = halves(sine(dot(w2s, jnp.concatenate([h1h, h1l, h1h], axis=0))))
+        h1h, h1l = halves(sine_of_turns(dot(w1s, fs)))
+        h2h, h2l = halves(sine_of_turns(dot(w2s, jnp.concatenate([h1h, h1l, h1h], axis=0))))
         values = dot(w3s, jnp.concatenate([h2h, h2l, h2h], axis=0))
         values = values * jnp.exp(-rates * tau)
         side_row = lax.broadcasted_iota(jnp.int32, values.shape, 0)
@@ -216,6 +216,8 @@
     total = lax.fori_loop(0, seq_len // chunk, step, jnp.zeros((2 * group, width), F32))
     power = jnp.sum(total, axis=1, keepdims=True)
     scale = lax.rsqrt(power[:group] + power[group:] + np.float32(1e-06))
+    for move in moves[5:]:
+        move.wait()
     cos, sin = twist[0], twist[1]
     cos2, sin2 = jnp.concatenate([cos, cos], axis=1), jnp.concatenate([sin, sin], axis=1)
     for c in range(group):
@@ -230,7 +232,17 @@
         high, low = halves(left)
         left_high[c * blocks : (c + 1) * blocks, :] = high
         left_low[c * blocks : (c + 1) * blocks, :] = low
-    out[...] = dot(left_high[...], both[0]) + dot(left_low[...], both[0]) + dot(left_high[...], both[1])
+    pieces = out_sems.shape[0]
+    size = group * blocks // pieces
+    writes = []
+    for n in range(pieces):
+        part = slice(n * size, (n + 1) * size)
+        high, low = left_high[part, :], left_low[part, :]
+        result[part, :] = dot(high, both[0]) + dot(low, both[0]) + dot(high, both[1])
+        writes.append(pltpu.make_async_copy(result.at[part, :], out.at[part, :], out_sems.at[n]))
+        writes[-1].start()
+    for write in writes:
+        write.wait()
 
 
 def conv_kernel(
@@ -358,16 +370,21 @@
     spec = pl.pallas_call(
         functools.partial(filter_kernel, seq_len=seq_len, width=width, chunk=4 * width, group=group),
         in_specs=[pl.BlockSpec(memory_space=pltpu.HBM)] * len(filter_args),
+        out_specs=pl.BlockSpec(memory_space=pltpu.HBM),
         out_shape=jax.ShapeDtypeStruct((group * cols, 2 * width), F32),
-        scratch_shapes=[pltpu.VMEM(x.shape, x.dtype) for x in filter_args]
+        scratch_shapes=[
+            pltpu.VMEM((x.shape[0], width) if n in (2, 3, 4) else x.shape, x.dtype) for n, x in enumerate(filter_args)
+        ]
         + [
             pltpu.VMEM((3, width, width), F32),
             pltpu.VMEM((2 * group * cols, width), F32),
             pltpu.VMEM((group * cols, 4 * width), BF16),
             pltpu.VMEM((group * cols, 4 * width), BF16),
+            pltpu.VMEM((group * cols, 2 * width), F32),
             pltpu.SemaphoreType.DMA((len(filter_args),)),
+            pltpu.SemaphoreType.DMA((4,)),
         ],
-        compiler_params=pltpu.CompilerParams(vmem_limit_bytes=ALL_VMEM),
+        compiler_params=pltpu.CompilerParams(vmem_limit_bytes=ALL_VMEM - 320 * 1024),
         cost_estimate=cost(10, 2**22),
         name="filter",
     )(*filter_args)

time: 147 us -> 142 us (0.966)
  Pallas kernels: 20.5 us -> 17.9 us
  blocking collectives: 24.5 us -> 22.3 us
  waiting for transfers between devices: 1.97 us -> 4.02 us
  local copies, waits for them, and re-layouts: 1.96 us -> 0.17 us
    all_to_all x1, blocking collectives: 24.5 us -> 22.3 us  [body(): lax.all_to_all(convolved.reshape(chips, CORES * group, width), CHIP, 0, 0...]
    all_to_all x1, waiting for transfers between devices: 0.01 us -> 2.05 us  [body(): plane = lax.all_to_all(product, CHIP, 0, 0, tiled=True)]
    pallas_call x1, Pallas kernels: 12.2 us -> 10.5 us  [body(): pl.pallas_call(functools.partial(filter_kernel, seq_len=seq_len, width=wi...]
  transfers between devices with their start and end apart: 3 -> 3, of which waited for: 2 -> 3; matrix products, arithmetic and copies ran while one was open for 0% -> 0% of each run, Pallas kernels for 8% -> 7%
where the time goes in v4:
time: 142 us
  starting transfers between devices  97.6 us (69%)
  blocking collectives  22.3 us (16%)
  Pallas kernels  17.9 us (13%)
  waiting for transfers between devices  4.02 us (3%)
    ppermute x1, starting transfers between devices, body(): lax.ppermute(lax.dynamic_slice_in_dim(plane, theirs_at, group + EDGE, 1),...  75.6 us
    all_to_all x1, blocking collectives, body(): lax.all_to_all(convolved.reshape(chips, CORES * group, width), CHIP, 0, 0...  22.3 us
    all_to_all x1, starting transfers between devices, body(): plane = lax.all_to_all(product, CHIP, 0, 0, tiled=True)  14.9 us
    pallas_call x1, Pallas kernels, body(): pl.pallas_call(functools.partial(filter_kernel, seq_len=seq_len, width=wi...  10.5 us
    ppermute x1, starting transfers between devices, body(): other = lax.ppermute(theirs, COL, swap)  7.06 us
    pallas_call x1, Pallas kernels, body(): pl.pallas_call(functools.partial(conv_kernel, group=group), out_shape=jax...  2.85 us
  transfers between devices with their start and end apart: 3, of which 3 were waited for; matrix products, arithmetic and copies ran while one was open for 0% of the time, Pallas kernels for 7%

profile of v4, /device:TPU:5, one launch (start us, length us, event | category | flops | bytes accessed | tf_op | source)
XLA Modules:
  0.0 142.2 jit_solution(5851211283243723921)
XLA Ops:
  0.0 2.3 %product.1 = bf16[16,72,128]{2,1,0:T(8,128)(2,1)} custom-call(bf16[128,1024]{1,0:T(8,128)(2,1)} %bitcast.10, bf16[128,1024]{1,0:T(8,128)(2,1)} %bitcast.12, bf16[128,1024]{1,0:T(8,128)(2,1)} %bitcast.7, bf16[128,1024]{1,0:T(8,128)(2,1)} %bitcast.8, f32[3,1024]{1,0:T(4,128)} %taps_mult.4, f32[3,1024]{1,0:T(4,128)} %taps_value.4), custom_call_target="tpu_custom_call" | custom-call | tf_op jit(solution)/shard_map/product/pallas_call | solution.py:350
  2.3 14.9 %all-to-all-start = ((bf16[16,72,128]{2,1,0:T(8,128)(2,1)}), bf16[16,72,128]{2,1,0:T(8,128)(2,1)S(1)}, u32[]{:S(2)}, u32[]{:S(2)}) async-start(bf16[16,72,128]{2,1,0:T(8,128)(2,1)} %product.1), calls=%async_computation | async-start | bytes 589824 | tf_op jit(solution)/shard_map/all_to_all | solution.py:366
  17.2 0.0 copy-start.4
  17.3 0.0 copy-start.5
  17.3 0.0 copy-start.6
  17.3 0.0 copy-start.7
  17.3 10.5 %filter.1.spec = f32[1024,256]{1,0:T(8,128)} custom-call(f32[33,128]{1,0:T(8,128)} %refs_0_.1, f32[128,128]{1,0:T(8,128)} %refs_1_.1, f32[128,1024]{1,0:T(8,128)} %refs_2_.1, f32[128,1024]{1,0:T(8,128)} %refs_3_.1, f32[1,1024]{1,0:T(1,128)} %bitcast.17, bf16[64,96]{1,0:T(8,128)(2,1)} %constant.24.clone.refs_5_, f32[2,32,128]{2,1,0:T(8,128)} %constant.25.clone.refs_6_.twist, ...), custom_call_target="tpu_custom_call" | custom-call | flops 4000000000 | bytes 4194304 | tf_op jit(solution)/shard_map/filter/pallas_call | solution.py:370
  27.8 0.0 copy-done.4
  27.8 0.0 copy-done.5
  27.8 0.0 copy-done.6
  27.8 0.0 copy-done.7
  27.8 0.0 copy-start.8
  27.9 0.0 copy-start.9
  27.9 0.0 copy-start.10
  27.9 0.0 copy-start.11
  27.9 0.0 copy-start.12
  27.9 0.0 copy-start.13
  27.9 0.1 gains.1
  28.0 0.0 copy-start.1
  28.0 0.0 copy-start.2
  28.0 0.0 copy-start.3
  28.0 2.0 %all-to-all-done.plane = bf16[16,72,128]{2,1,0:T(8,128)(2,1)S(1)} async-done(((bf16[16,72,128]{2,1,0:T(8,128)(2,1)}), bf16[16,72,128]{2,1,0:T(8,128)(2,1)S(1)}, u32[]{:S(2)}, u32[]{:S(2)}) %all-to-all-start) | async-done | bytes 294944 | tf_op jit(solution)/shard_map/all_to_all | solution.py:366
  30.1 0.0 copy-start
  30.1 0.1 constant_dynamic-slice_fusion.1
  30.1 75.6 %collective-permute-start = (bf16[16,40,128]{2,1,0:T(8,128)(2,1)S(1)}, bf16[16,40,128]{2,1,0:T(8,128)(2,1)S(1)}, u32[]{:S(2)}, u32[]{:S(2)}) collective-permute-start(bf16[16,40,128]{2,1,0:T(8,128)(2,1)S(1)} %constant_dynamic-slice_fusion.1), channel_id=1, source_target_pairs={{0,1},{1,0},{2,3},{3,2},{4,5},{5,4},{6,7},{7,6},{8,9},{9,8},{10,11... | collective-permute-start | bytes 491528 | tf_op jit(solution)/shard_map/ppermute | solution.py:400
  105.7 1.0 collective-permute-done.partner
  106.7 0.0 copy-done.8
  106.7 0.0 copy-done.9
  106.7 0.0 copy-done.10
  106.7 0.0 copy-done.11
  106.7 0.0 copy-done.12
  106.7 0.0 copy-done.13
  106.8 2.8 %conv.1 = bf16[1024,128]{1,0:T(8,128)(2,1)S(1)} custom-call(bf16[16,72,128]{2,1,0:T(8,128)(2,1)S(1)} %all-to-all-done.plane, bf16[16,40,128]{2,1,0:T(8,128)(2,1)S(1)} %collective-permute-done.partner, f32[16,128]{1,0:T(8,128)S(1)} %gains.1, f32[1024,256]{1,0:T(8,128)S(1)} %copy-done.13, bf16[64,64]{1,0:T(8,128)(2,1)S(1)} %copy-done.12, ...), custom_call_target="tpu_custom_call" | custom-call | flops 1200000000 | bytes 2097152 | tf_op jit(solution)/shard_map/conv/pallas_call | solution.py:402
  109.6 22.3 %all_to_all.10.planes = bf16[16,64,128]{2,1,0:T(8,128)(2,1)S(1)} all-to-all(bf16[16,64,128]{2,1,0:T(8,128)(2,1)S(1)} %bitcast.14), channel_id=1, replica_groups=mesh['grp'=2,'row'=16,'col_chip'=16,'col_core'=2] {'col_chip'}, dimensions={0} | all-to-all | bytes 524288 | tf_op jit(solution)/shard_map/all_to_all | solution.py:415
  131.9 7.1 %collective-permute-start.1 = (bf16[16,32,128]{2,1,0:T(8,128)(2,1)S(1)}, bf16[16,32,128]{2,1,0:T(8,128)(2,1)S(1)}, u32[]{:S(2)}, u32[]{:S(2)}) collective-permute-start(bf16[16,32,128]{2,1,0:T(8,128)(2,1)S(1)} %constant_dynamic-slice_fusion), channel_id=1, source_target_pairs={{0,1},{1,0},{2,3},{3,2},{4,5},{5,4},{6,7},{7,6},{8,9},{9,8},{10,11... | collective-permute-start | bytes 393224 | tf_op jit(solution)/shard_map/ppermute | solution.py:417
  139.0 1.0 collective-permute-done.1.other
  140.0 0.0 copy-done.1
  140.0 0.0 copy-done.2
  140.0 0.0 copy-done.3
  140.0 0.0 copy-done
  140.0 2.2 %mix.1 = bf16[128,2048]{1,0:T(8,128)(2,1)} custom-call(bf16[16,64,128]{2,1,0:T(8,128)(2,1)S(1)} %all_to_all.10.planes, bf16[16,32,128]{2,1,0:T(8,128)(2,1)S(1)} %collective-permute-done.1.other, bf16[128,1024]{1,0:T(8,128)(2,1)S(1)} %bitcast.9, bf16[128,1024]{1,0:T(8,128)(2,1)S(1)} %bitcast.11, bf16[128,1024]{1,0:T(8,128)(2,1)S(1)} %bitcast.13, ...), custom_call_target="tpu_custom_call" | custom-call | flops 800000000 | bytes 4194304 | tf_op jit(solution)/shard_map/mix/pallas_call | solution.py:418
  (1 shorter events, 0.0 us)
Async XLA Ops:
  2.3 27.8 %all-to-all-start = ((bf16[16,72,128]{2,1,0:T(8,128)(2,1)}), bf16[16,72,128]{2,1,0:T(8,128)(2,1)S(1)}, u32[]{:S(2)}, u32[]{:S(2)}) async-start(bf16[16,72,128]{2,1,0:T(8,128)(2,1)} %product.1), calls=%async_computation | async-start | bytes 589824 | tf_op jit(solution)/shard_map/all_to_all | solution.py:366
  17.2 10.6 %copy-start.4 = (f32[3,1024]{1,0:T(4,128)S(1)}, f32[3,1024]{1,0:T(4,128)}, u32[]{:S(2)}) copy-start(f32[3,1024]{1,0:T(4,128)} %taps_mult.4) | copy-start | bytes 36868
  17.3 10.6 %copy-start.5 = (f32[3,1024]{1,0:T(4,128)S(1)}, f32[3,1024]{1,0:T(4,128)}, u32[]{:S(2)}) copy-start(f32[3,1024]{1,0:T(4,128)} %taps_value.4) | copy-start | bytes 36868
  17.3 10.6 %copy-start.6 = (f32[3,1024]{1,0:T(4,128)S(1)}, f32[3,1024]{1,0:T(4,128)}, u32[]{:S(2)}) copy-start(f32[3,1024]{1,0:T(4,128)} %taps_gate.2) | copy-start | bytes 36868
  17.3 10.6 %copy-start.7 = (f32[1024]{0:T(1024)S(1)}, f32[1024]{0:T(1024)}, u32[]{:S(2)}) copy-start(f32[1024]{0:T(1024)} %param.31) | copy-start | bytes 12292
  27.8 78.9 %copy-start.8 = (bf16[2,256,256]{2,1,0:T(8,128)(2,1)S(1)}, bf16[2,256,256]{2,1,0:T(8,128)(2,1)}, u32[]{:S(2)}) copy-start(bf16[2,256,256]{2,1,0:T(8,128)(2,1)} %constant.29.clone.back) | copy-start | bytes 786436
  27.9 78.9 %copy-start.9 = (bf16[2,256,256]{2,1,0:T(8,128)(2,1)S(1)}, bf16[2,256,256]{2,1,0:T(8,128)(2,1)}, u32[]{:S(2)}) copy-start(bf16[2,256,256]{2,1,0:T(8,128)(2,1)} %constant.28.clone.ahead) | copy-start | bytes 786436
  27.9 78.9 %copy-start.10 = (f32[2,32,128]{2,1,0:T(8,128)S(1)}, f32[2,32,128]{2,1,0:T(8,128)}, u32[]{:S(2)}) copy-start(f32[2,32,128]{2,1,0:T(8,128)} %constant.25.clone.refs_6_.twist) | copy-start | bytes 98308
  27.9 78.8 %copy-start.11 = (bf16[32,192]{1,0:T(8,128)(2,1)S(1)}, bf16[32,192]{1,0:T(8,128)(2,1)}, u32[]{:S(2)}) copy-start(bf16[32,192]{1,0:T(8,128)(2,1)} %constant.30.clone.last) | copy-start | bytes 36868
  27.9 78.8 %copy-start.12 = (bf16[64,64]{1,0:T(8,128)(2,1)S(1)}, bf16[64,64]{1,0:T(8,128)(2,1)}, u32[]{:S(2)}) copy-start(bf16[64,64]{1,0:T(8,128)(2,1)} %constant.27.clone.data_first) | copy-start | bytes 24580
  27.9 78.8 %copy-start.13 = (f32[1024,256]{1,0:T(8,128)S(1)}, f32[1024,256]{1,0:T(8,128)}, u32[]{:S(2)}) copy-start(f32[1024,256]{1,0:T(8,128)} %filter.1.spec) | copy-start | bytes 3145732
  28.0 112.0 %copy-start.1 = (bf16[1,128,1024]{2,1,0:T(8,128)(2,1)S(1)}, bf16[1,128,1024]{2,1,0:T(8,128)(2,1)}, u32[]{:S(2)}) copy-start(bf16[1,128,1024]{2,1,0:T(8,128)(2,1)} %param.20) | copy-start | bytes 786436
  28.0 112.0 %copy-start.2 = (bf16[1,128,1024]{2,1,0:T(8,128)(2,1)S(1)}, bf16[1,128,1024]{2,1,0:T(8,128)(2,1)}, u32[]{:S(2)}) copy-start(bf16[1,128,1024]{2,1,0:T(8,128)(2,1)} %param.21) | copy-start | bytes 786436
  28.0 112.0 %copy-start.3 = (bf16[1,128,1024]{2,1,0:T(8,128)(2,1)S(1)}, bf16[1,128,1024]{2,1,0:T(8,128)(2,1)}, u32[]{:S(2)}) copy-start(bf16[1,128,1024]{2,1,0:T(8,128)(2,1)} %param.22) | copy-start | bytes 786436
  30.1 109.9 %copy-start = (bf16[1024,2048]{1,0:T(8,128)(2,1)S(1)}, bf16[1024,2048]{1,0:T(8,128)(2,1)}, u32[]{:S(2)}) copy-start(bf16[1024,2048]{1,0:T(8,128)(2,1)} %weight.1) | copy-start | bytes 12582916
  30.1 76.6 %collective-permute-start = (bf16[16,40,128]{2,1,0:T(8,128)(2,1)S(1)}, bf16[16,40,128]{2,1,0:T(8,128)(2,1)S(1)}, u32[]{:S(2)}, u32[]{:S(2)}) collective-permute-start(bf16[16,40,128]{2,1,0:T(8,128)(2,1)S(1)} %constant_dynamic-slice_fusion.1), channel_id=1, source_target_pairs={{0,1},{1,0},{2,3},{3,2},{4,5},{5,4},{6,7},{7,6},{8,9},{9,8},{10,11... | collective-permute-start | bytes 491528 | tf_op jit(solution)/shard_map/ppermute | solution.py:400
  131.9 8.0 %collective-permute-start.1 = (bf16[16,32,128]{2,1,0:T(8,128)(2,1)S(1)}, bf16[16,32,128]{2,1,0:T(8,128)(2,1)S(1)}, u32[]{:S(2)}, u32[]{:S(2)}) collective-permute-start(bf16[16,32,128]{2,1,0:T(8,128)(2,1)S(1)} %constant_dynamic-slice_fusion), channel_id=1, source_target_pairs={{0,1},{1,0},{2,3},{3,2},{4,5},{5,4},{6,7},{7,6},{8,9},{9,8},{10,11... | collective-permute-start | bytes 393224 | tf_op jit(solution)/shard_map/ppermute | solution.py:417

commit v5 on v4

--- a/solution.py
+++ b/solution.py
@@ -368,7 +368,7 @@
         filter_first, filter_second, filter_ahead, filter_behind, filter_decay[None], t["kernel_first"], t["twist"], t["both"]
     )
     spec = pl.pallas_call(
-        functools.partial(filter_kernel, seq_len=seq_len, width=width, chunk=4 * width, group=group),
+        functools.partial(filter_kernel, seq_len=seq_len, width=width, chunk=16 * width, group=group),
         in_specs=[pl.BlockSpec(memory_space=pltpu.HBM)] * len(filter_args),
         out_specs=pl.BlockSpec(memory_space=pltpu.HBM),
         out_shape=jax.ShapeDtypeStruct((group * cols, 2 * width), F32),

time: 142 us -> 140 us (0.986)
  waiting for transfers between devices: 4.02 us -> 7.04 us
  Pallas kernels: 17.9 us -> 14.9 us
  blocking collectives: 22.3 us -> 20.1 us
    all_to_all x1, waiting for transfers between devices: 2.05 us -> 5.07 us  [body(): plane = lax.all_to_all(product, CHIP, 0, 0, tiled=True)]
    pallas_call x1, Pallas kernels: 10.5 us -> 7.48 us  [body(): pl.pallas_call(functools.partial(filter_kernel, seq_len=seq_len, width=wi...]
    all_to_all x1, blocking collectives: 22.3 us -> 20.1 us  [body(): lax.all_to_all(convolved.reshape(chips, CORES * group, width), CHIP, 0, 0...]
  transfers between devices with their start and end apart: 3 -> 3, of which waited for: 3 -> 3; matrix products, arithmetic and copies ran while one was open for 0% -> 0% of each run, Pallas kernels for 7% -> 5%
where the time goes in v5:
time: 140 us
  starting transfers between devices  97.6 us (70%)
  blocking collectives  20.1 us (14%)
  Pallas kernels  14.9 us (11%)
  waiting for transfers between devices  7.04 us (5%)
    ppermute x1, starting transfers between devices, body(): lax.ppermute(lax.dynamic_slice_in_dim(plane, theirs_at, group + EDGE, 1),...  75.6 us
    all_to_all x1, blocking collectives, body(): lax.all_to_all(convolved.reshape(chips, CORES * group, width), CHIP, 0, 0...  20.1 us
    all_to_all x1, starting transfers between devices, body(): plane = lax.all_to_all(product, CHIP, 0, 0, tiled=True)  14.9 us
    pallas_call x1, Pallas kernels, body(): pl.pallas_call(functools.partial(filter_kernel, seq_len=seq_len, width=wi...  7.48 us
    ppermute x1, starting transfers between devices, body(): other = lax.ppermute(theirs, COL, swap)  7.08 us
    all_to_all x1, waiting for transfers between devices, body(): plane = lax.all_to_all(product, CHIP, 0, 0, tiled=True)  5.07 us
    pallas_call x1, Pallas kernels, body(): pl.pallas_call(functools.partial(conv_kernel, group=group), out_shape=jax...  2.85 us
  transfers between devices with their start and end apart: 3, of which 3 were waited for; matrix products, arithmetic and copies ran while one was open for 0% of the time, Pallas kernels for 5%

profile of v5, /device:TPU:5, one launch (start us, length us, event | category | flops | bytes accessed | tf_op | source)
XLA Modules:
  0.0 140.0 jit_solution(17418203609802440911)
XLA Ops:
  0.0 2.3 %product.1 = bf16[16,72,128]{2,1,0:T(8,128)(2,1)} custom-call(bf16[128,1024]{1,0:T(8,128)(2,1)} %bitcast.10, bf16[128,1024]{1,0:T(8,128)(2,1)} %bitcast.12, bf16[128,1024]{1,0:T(8,128)(2,1)} %bitcast.7, bf16[128,1024]{1,0:T(8,128)(2,1)} %bitcast.8, f32[3,1024]{1,0:T(4,128)} %taps_mult.4, f32[3,1024]{1,0:T(4,128)} %taps_value.4), custom_call_target="tpu_custom_call" | custom-call | tf_op jit(solution)/shard_map/product/pallas_call | solution.py:350
  2.3 14.9 %all-to-all-start = ((bf16[16,72,128]{2,1,0:T(8,128)(2,1)}), bf16[16,72,128]{2,1,0:T(8,128)(2,1)S(1)}, u32[]{:S(2)}, u32[]{:S(2)}) async-start(bf16[16,72,128]{2,1,0:T(8,128)(2,1)} %product.1), calls=%async_computation | async-start | bytes 589824 | tf_op jit(solution)/shard_map/all_to_all | solution.py:366
  17.2 0.0 copy-start.4
  17.3 0.0 copy-start.5
  17.3 0.0 copy-start.6
  17.3 0.0 copy-start.7
  17.3 7.5 %filter.1.spec = f32[1024,256]{1,0:T(8,128)} custom-call(f32[33,128]{1,0:T(8,128)} %refs_0_.1, f32[128,128]{1,0:T(8,128)} %refs_1_.1, f32[128,1024]{1,0:T(8,128)} %refs_2_.1, f32[128,1024]{1,0:T(8,128)} %refs_3_.1, f32[1,1024]{1,0:T(1,128)} %bitcast.17, bf16[64,96]{1,0:T(8,128)(2,1)} %constant.24.clone.refs_5_, f32[2,32,128]{2,1,0:T(8,128)} %constant.25.clone.refs_6_.twist, ...), custom_call_target="tpu_custom_call" | custom-call | flops 4000000000 | bytes 4194304 | tf_op jit(solution)/shard_map/filter/pallas_call | solution.py:370
  24.8 0.0 copy-done.4
  24.8 0.0 copy-done.5
  24.8 0.0 copy-done.6
  24.8 0.0 copy-done.7
  24.8 0.0 copy-start.8
  24.8 0.0 copy-start.9
  24.8 0.0 copy-start.10
  24.9 0.0 copy-start.11
  24.9 0.0 copy-start.12
  24.9 0.0 copy-start.13
  24.9 0.1 gains.1
  25.0 0.0 copy-start.1
  25.0 0.0 copy-start.2
  25.0 0.0 copy-start.3
  25.0 5.1 %all-to-all-done.plane = bf16[16,72,128]{2,1,0:T(8,128)(2,1)S(1)} async-done(((bf16[16,72,128]{2,1,0:T(8,128)(2,1)}), bf16[16,72,128]{2,1,0:T(8,128)(2,1)S(1)}, u32[]{:S(2)}, u32[]{:S(2)}) %all-to-all-start) | async-done | bytes 294944 | tf_op jit(solution)/shard_map/all_to_all | solution.py:366
  30.1 0.0 copy-start
  30.1 0.1 constant_dynamic-slice_fusion.1
  30.1 75.6 %collective-permute-start = (bf16[16,40,128]{2,1,0:T(8,128)(2,1)S(1)}, bf16[16,40,128]{2,1,0:T(8,128)(2,1)S(1)}, u32[]{:S(2)}, u32[]{:S(2)}) collective-permute-start(bf16[16,40,128]{2,1,0:T(8,128)(2,1)S(1)} %constant_dynamic-slice_fusion.1), channel_id=1, source_target_pairs={{0,1},{1,0},{2,3},{3,2},{4,5},{5,4},{6,7},{7,6},{8,9},{9,8},{10,11... | collective-permute-start | bytes 491528 | tf_op jit(solution)/shard_map/ppermute | solution.py:400
  105.7 1.0 collective-permute-done.partner
  106.7 0.0 copy-done.8
  106.7 0.0 copy-done.9
  106.7 0.0 copy-done.10
  106.7 0.0 copy-done.11
  106.7 0.0 copy-done.12
  106.7 0.0 copy-done.13
  106.8 2.8 %conv.1 = bf16[1024,128]{1,0:T(8,128)(2,1)S(1)} custom-call(bf16[16,72,128]{2,1,0:T(8,128)(2,1)S(1)} %all-to-all-done.plane, bf16[16,40,128]{2,1,0:T(8,128)(2,1)S(1)} %collective-permute-done.partner, f32[16,128]{1,0:T(8,128)S(1)} %gains.1, f32[1024,256]{1,0:T(8,128)S(1)} %copy-done.13, bf16[64,64]{1,0:T(8,128)(2,1)S(1)} %copy-done.12, ...), custom_call_target="tpu_custom_call" | custom-call | flops 1200000000 | bytes 2097152 | tf_op jit(solution)/shard_map/conv/pallas_call | solution.py:402
  109.6 20.1 %all_to_all.10.planes = bf16[16,64,128]{2,1,0:T(8,128)(2,1)S(1)} all-to-all(bf16[16,64,128]{2,1,0:T(8,128)(2,1)S(1)} %bitcast.14), channel_id=1, replica_groups=mesh['grp'=2,'row'=16,'col_chip'=16,'col_core'=2] {'col_chip'}, dimensions={0} | all-to-all | bytes 524288 | tf_op jit(solution)/shard_map/all_to_all | solution.py:415
  129.8 7.1 %collective-permute-start.1 = (bf16[16,32,128]{2,1,0:T(8,128)(2,1)S(1)}, bf16[16,32,128]{2,1,0:T(8,128)(2,1)S(1)}, u32[]{:S(2)}, u32[]{:S(2)}) collective-permute-start(bf16[16,32,128]{2,1,0:T(8,128)(2,1)S(1)} %constant_dynamic-slice_fusion), channel_id=1, source_target_pairs={{0,1},{1,0},{2,3},{3,2},{4,5},{5,4},{6,7},{7,6},{8,9},{9,8},{10,11... | collective-permute-start | bytes 393224 | tf_op jit(solution)/shard_map/ppermute | solution.py:417
  136.8 1.0 collective-permute-done.1.other
  137.8 0.0 copy-done.1
  137.8 0.0 copy-done.2
  137.8 0.0 copy-done.3
  137.8 0.0 copy-done
  137.8 2.2 %mix.1 = bf16[128,2048]{1,0:T(8,128)(2,1)} custom-call(bf16[16,64,128]{2,1,0:T(8,128)(2,1)S(1)} %all_to_all.10.planes, bf16[16,32,128]{2,1,0:T(8,128)(2,1)S(1)} %collective-permute-done.1.other, bf16[128,1024]{1,0:T(8,128)(2,1)S(1)} %bitcast.9, bf16[128,1024]{1,0:T(8,128)(2,1)S(1)} %bitcast.11, bf16[128,1024]{1,0:T(8,128)(2,1)S(1)} %bitcast.13, ...), custom_call_target="tpu_custom_call" | custom-call | flops 800000000 | bytes 4194304 | tf_op jit(solution)/shard_map/mix/pallas_call | solution.py:418
  (1 shorter events, 0.0 us)
Async XLA Ops:
  2.3 27.8 %all-to-all-start = ((bf16[16,72,128]{2,1,0:T(8,128)(2,1)}), bf16[16,72,128]{2,1,0:T(8,128)(2,1)S(1)}, u32[]{:S(2)}, u32[]{:S(2)}) async-start(bf16[16,72,128]{2,1,0:T(8,128)(2,1)} %product.1), calls=%async_computation | async-start | bytes 589824 | tf_op jit(solution)/shard_map/all_to_all | solution.py:366
  17.2 7.5 %copy-start.4 = (f32[3,1024]{1,0:T(4,128)S(1)}, f32[3,1024]{1,0:T(4,128)}, u32[]{:S(2)}) copy-start(f32[3,1024]{1,0:T(4,128)} %taps_mult.4) | copy-start | bytes 36868
  17.3 7.5 %copy-start.5 = (f32[3,1024]{1,0:T(4,128)S(1)}, f32[3,1024]{1,0:T(4,128)}, u32[]{:S(2)}) copy-start(f32[3,1024]{1,0:T(4,128)} %taps_value.4) | copy-start | bytes 36868
  17.3 7.5 %copy-start.6 = (f32[3,1024]{1,0:T(4,128)S(1)}, f32[3,1024]{1,0:T(4,128)}, u32[]{:S(2)}) copy-start(f32[3,1024]{1,0:T(4,128)} %taps_gate.2) | copy-start | bytes 36868
  17.3 7.5 %copy-start.7 = (f32[1024]{0:T(1024)S(1)}, f32[1024]{0:T(1024)}, u32[]{:S(2)}) copy-start(f32[1024]{0:T(1024)} %param.31) | copy-start | bytes 12292
  24.8 81.9 %copy-start.8 = (bf16[2,256,256]{2,1,0:T(8,128)(2,1)S(1)}, bf16[2,256,256]{2,1,0:T(8,128)(2,1)}, u32[]{:S(2)}) copy-start(bf16[2,256,256]{2,1,0:T(8,128)(2,1)} %constant.29.clone.back) | copy-start | bytes 786436
  24.8 81.9 %copy-start.9 = (bf16[2,256,256]{2,1,0:T(8,128)(2,1)S(1)}, bf16[2,256,256]{2,1,0:T(8,128)(2,1)}, u32[]{:S(2)}) copy-start(bf16[2,256,256]{2,1,0:T(8,128)(2,1)} %constant.28.clone.ahead) | copy-start | bytes 786436
  24.8 81.9 %copy-start.10 = (f32[2,32,128]{2,1,0:T(8,128)S(1)}, f32[2,32,128]{2,1,0:T(8,128)}, u32[]{:S(2)}) copy-start(f32[2,32,128]{2,1,0:T(8,128)} %constant.25.clone.refs_6_.twist) | copy-start | bytes 98308
  24.9 81.9 %copy-start.11 = (bf16[32,192]{1,0:T(8,128)(2,1)S(1)}, bf16[32,192]{1,0:T(8,128)(2,1)}, u32[]{:S(2)}) copy-start(bf16[32,192]{1,0:T(8,128)(2,1)} %constant.30.clone.last) | copy-start | bytes 36868
  24.9 81.9 %copy-start.12 = (bf16[64,64]{1,0:T(8,128)(2,1)S(1)}, bf16[64,64]{1,0:T(8,128)(2,1)}, u32[]{:S(2)}) copy-start(bf16[64,64]{1,0:T(8,128)(2,1)} %constant.27.clone.data_first) | copy-start | bytes 24580
  24.9 81.9 %copy-start.13 = (f32[1024,256]{1,0:T(8,128)S(1)}, f32[1024,256]{1,0:T(8,128)}, u32[]{:S(2)}) copy-start(f32[1024,256]{1,0:T(8,128)} %filter.1.spec) | copy-start | bytes 3145732
  25.0 112.8 %copy-start.1 = (bf16[1,128,1024]{2,1,0:T(8,128)(2,1)S(1)}, bf16[1,128,1024]{2,1,0:T(8,128)(2,1)}, u32[]{:S(2)}) copy-start(bf16[1,128,1024]{2,1,0:T(8,128)(2,1)} %param.20) | copy-start | bytes 786436
  25.0 112.8 %copy-start.2 = (bf16[1,128,1024]{2,1,0:T(8,128)(2,1)S(1)}, bf16[1,128,1024]{2,1,0:T(8,128)(2,1)}, u32[]{:S(2)}) copy-start(bf16[1,128,1024]{2,1,0:T(8,128)(2,1)} %param.21) | copy-start | bytes 786436
  25.0 112.8 %copy-start.3 = (bf16[1,128,1024]{2,1,0:T(8,128)(2,1)S(1)}, bf16[1,128,1024]{2,1,0:T(8,128)(2,1)}, u32[]{:S(2)}) copy-start(bf16[1,128,1024]{2,1,0:T(8,128)(2,1)} %param.22) | copy-start | bytes 786436
  30.1 107.8 %copy-start = (bf16[1024,2048]{1,0:T(8,128)(2,1)S(1)}, bf16[1024,2048]{1,0:T(8,128)(2,1)}, u32[]{:S(2)}) copy-start(bf16[1024,2048]{1,0:T(8,128)(2,1)} %weight.1) | copy-start | bytes 12582916
  30.1 76.6 %collective-permute-start = (bf16[16,40,128]{2,1,0:T(8,128)(2,1)S(1)}, bf16[16,40,128]{2,1,0:T(8,128)(2,1)S(1)}, u32[]{:S(2)}, u32[]{:S(2)}) collective-permute-start(bf16[16,40,128]{2,1,0:T(8,128)(2,1)S(1)} %constant_dynamic-slice_fusion.1), channel_id=1, source_target_pairs={{0,1},{1,0},{2,3},{3,2},{4,5},{5,4},{6,7},{7,6},{8,9},{9,8},{10,11... | collective-permute-start | bytes 491528 | tf_op jit(solution)/shard_map/ppermute | solution.py:400
  129.8 8.0 %collective-permute-start.1 = (bf16[16,32,128]{2,1,0:T(8,128)(2,1)S(1)}, bf16[16,32,128]{2,1,0:T(8,128)(2,1)S(1)}, u32[]{:S(2)}, u32[]{:S(2)}) collective-permute-start(bf16[16,32,128]{2,1,0:T(8,128)(2,1)S(1)} %constant_dynamic-slice_fusion), channel_id=1, source_target_pairs={{0,1},{1,0},{2,3},{3,2},{4,5},{5,4},{6,7},{7,6},{8,9},{9,8},{10,11... | collective-permute-start | bytes 393224 | tf_op jit(solution)/shard_map/ppermute | solution.py:417
